TPU v7x, 512 devices: a whole 4x4x16 slice. The times are simulated.
512 devices in a mesh: fs: 128 (over z, x, core), tp: 4 (over y).
Axes of the slice: x: 4, y: 4, z: 16, core: 2. Of those that a mesh axis runs over, the one named last changes fastest.
Arguments:
- tokens: bfloat16 [16384, 2048], P('fs'), may hold values from -6 to 6
- gain: float32 [2048], P('fs'), may hold values from 0.1 to 1.9
- up_master: float32 [2048, 8192], P('fs', 'tp'), may hold values from -0.125 to 0.125
- down_master: float32 [2048, 8192], P('fs', 'tp'), may hold values from -0.0625 to 0.0625
Outputs:
- up_sampled: bfloat16 [128, 2048, 1024], P('fs', None, 'tp')
- down_sampled: bfloat16 [128, 2048, 1024], P('fs', None, 'tp')
- mixed: bfloat16 [16384, 2048], P('fs', 'tp')
All inputs are finite; a program needn't handle non-finite values.
Results may differ from a plain program's by a relative error of at most 0.0087.
Values may be sent and summed in bfloat16 or wider, within the bound.
No kernel may reach another device: no remote copies, remote signals or barrier semaphores. Data moves between devices by JAX's collectives and lax.ppermute only.
A program may use at most 64 MiB of HBM per device.

v0:
```python
import jax
import jax.numpy as jnp
from jax import lax
from jax.sharding import PartitionSpec as P

SUB = 8


def sent_together(arrays, axis, split_dim, concat_dim, along):
    widths = [a.shape[along] for a in arrays]
    both = jnp.concatenate(arrays, axis=along)
    out = lax.all_to_all(both, axis, split_axis=split_dim, concat_axis=concat_dim, tiled=True)
    return tuple(jnp.split(out, [sum(widths[:k]) for k in range(1, len(widths))], axis=along))


def from_partner(block, axis, bit):
    count = lax.axis_size(axis)
    route = []
    for low in range(count):
        high = low | 1 << bit
        if high != low and high < count:
            route += [(low, high), (high, low)]
    return lax.ppermute(block, axis, route)


def in_blocks(array, dim, devices):
    dims = array.shape
    pieces = array.reshape(*dims[:dim], devices, dims[dim] // devices, *dims[dim + 1 :])
    return jnp.moveaxis(pieces, dim, 0)


def sum_at_owner(array, axis, dim):
    devices = lax.axis_size(axis)
    pieces = lax.all_to_all(in_blocks(array, dim, devices), axis, 0, 0, tiled=True)
    return jnp.sum(pieces.astype(jnp.float32), axis=0)


def on_device(tokens, gain, up_master, down_master):
    fs_count = lax.axis_size("fs")
    feat_rows = up_master.shape[0]
    units = up_master.shape[1] // SUB
    groups_count = fs_count // SUB
    member = lax.axis_index("fs") % SUB
    up_round = (gain[:, None] * up_master).astype(jnp.bfloat16)
    down_round = down_master.astype(jnp.bfloat16)

    def spread(weight):
        blocks = weight.reshape(feat_rows, SUB, units).transpose(1, 0, 2)
        return jnp.broadcast_to(blocks[None], (groups_count, SUB, feat_rows, units)).reshape(
            fs_count, feat_rows, units
        )

    up_sampled, down_sampled = sent_together((spread(up_round), spread(down_round)), "fs", 0, 1, 2)
    levels = SUB.bit_length() - 1
    bit_list = list(range(levels))
    widened = tokens.astype(jnp.float32)
    normed = (
        widened * lax.rsqrt(jnp.mean(widened * widened, axis=1, keepdims=True) + 1e-06)
    ).astype(jnp.bfloat16)
    current = normed[None]
    for bit in bit_list:
        partner = from_partner(current, "fs", bit)
        lower = member >> bit & 1 == 0
        current = jnp.where(lower, jnp.stack([current, partner]), jnp.stack([partner, current]))
    order_now = list(reversed(bit_list))
    wanted = list(range(levels - 1, -1, -1))
    perm_axes = [
        [place for place, value in enumerate(order_now) if value == target][0] for target in wanted
    ]
    current = jnp.transpose(current, perm_axes + [levels, levels + 1, levels + 2])
    gathered = current.reshape(SUB * tokens.shape[0], tokens.shape[1])
    pre_units = jnp.dot(gathered, up_sampled[0], preferred_element_type=jnp.float32)
    act_units = jnp.square(jax.nn.relu(pre_units)).astype(jnp.bfloat16)
    partial_out = lax.dot_general(
        act_units, down_sampled[0], (((1,), (1,)), ((), ())), preferred_element_type=jnp.float32
    )
    running = partial_out.reshape((2,) * levels + (tokens.shape[0], tokens.shape[1]))
    axis_bits = list(range(levels - 1, -1, -1))
    for bit in bit_list:
        position = len([value for value in axis_bits if value > bit])
        mine = member >> bit & 1
        keep = lax.dynamic_index_in_dim(running, mine, position, keepdims=False)
        other = lax.dynamic_index_in_dim(running, 1 - mine, position, keepdims=False)
        running = keep + from_partner(other.astype(jnp.bfloat16), "fs", bit).astype(other.dtype)
        axis_bits = [value for value in axis_bits if value != bit]
    summed = sum_at_owner(running.astype(jnp.bfloat16), "tp", 1)
    return (up_sampled, down_sampled, summed.astype(jnp.bfloat16))


def solution(mesh):
    placed = (P("fs", None), P("fs"), P("fs", "tp"), P("fs", "tp"))
    return jax.shard_map(
        on_device,
        mesh=mesh,
        in_specs=placed,
        out_specs=(P("fs", None, "tp"), P("fs", None, "tp"), P("fs", "tp")),
        check_vma=False,
    )
```

profile of v0, /device:TPU:1, one launch (start us, length us, event | category | flops | bytes accessed | tf_op | source)
XLA Modules:
  0.0 213.3 jit_solution(3655158241734911424)
XLA Ops:
  2.8 1.6 pad_maximum_fusion
  4.4 20.5 %all-to-all-start = ((bf16[128,16,512]{2,1,0:T(8,128)(2,1)}), bf16[128,16,512]{2,1,0:T(8,128)(2,1)S(1)}, u32[]{:S(2)}, u32[]{:S(2)}) async-start(bf16[128,16,512]{2,1,0:T(8,128)(2,1)} %pad_maximum_fusion), calls=%async_computation | async-start | bytes 4194304 | tf_op jit(solution)/shard_map/all_to_all | solution.py:12
  26.1 2.8 %collective-permute-start = (bf16[1,128,2048]{2,1,0:T(8,128)(2,1)}, bf16[1,128,2048]{2,1,0:T(8,128)(2,1)S(1)}, u32[]{:S(2)}, u32[]{:S(2)}) collective-permute-start(bf16[1,128,2048]{2,1,0:T(8,128)(2,1)} %get-tuple-element.8), channel_id=1, source_target_pairs={{0,4},{4,0},{8,12},{12,8},{16,20},{20,16},{24,28},{28,24},{32,36},... | collective-permute-start | bytes 1572872 | tf_op jit(solution)/shard_map/ppermute | solution.py:23
  28.9 1.7 collective-permute-done
  31.8 2.8 %collective-permute-start.1 = (bf16[2,1,128,2048]{3,2,1,0:T(8,128)(2,1)}, bf16[2,1,128,2048]{3,2,1,0:T(8,128)(2,1)}, u32[]{:S(2)}, u32[]{:S(2)}) collective-permute-start(bf16[2,1,128,2048]{3,2,1,0:T(8,128)(2,1)} %maximum_select_fusion.4), channel_id=1, source_target_pairs={{0,8},{8,0},{4,12},{12,4},{16,24},{24,16},{20,28},{28,20},{32,40},... | collective-permute-start | bytes 3145736 | tf_op jit(solution)/shard_map/ppermute | solution.py:23
  35.7 29.8 %collective-permute-done.1 = bf16[2,1,128,2048]{3,2,1,0:T(8,128)(2,1)} collective-permute-done((bf16[2,1,128,2048]{3,2,1,0:T(8,128)(2,1)}, bf16[2,1,128,2048]{3,2,1,0:T(8,128)(2,1)}, u32[]{:S(2)}, u32[]{:S(2)}) %collective-permute-start.1) | collective-permute-done | bytes 1048608 | tf_op jit(solution)/shard_map/ppermute | solution.py:23
  65.5 3.3 %maximum_select_fusion.2 = bf16[2,2,1,128,2048]{4,3,1,2,0:T(8,128)(2,1)} fusion(bf16[1,2,1,128,2048]{4,3,1,2,0:T(8,128)(2,1)} %bitcast.12, bf16[1,2,1,128,2048]{4,3,1,2,0:T(8,128)(2,1)S(1)} %get-tuple-element.6, pred[]{:T(512)S(6)} %eq.12), kind=kLoop, calls=%fused_computation.7 | loop fusion | flops 3145728 | bytes 4194305 | tf_op jit(solution)/shard_map/jit(_where)/select_n | solution.py:64
  68.8 3.6 %collective-permute-start.2 = (bf16[2,2,1,128,2048]{4,3,1,2,0:T(8,128)(2,1)}, bf16[2,2,1,128,2048]{4,3,1,2,0:T(8,128)(2,1)}, u32[]{:S(2)}, u32[]{:S(2)}) collective-permute-start(bf16[2,2,1,128,2048]{4,3,1,2,0:T(8,128)(2,1)} %maximum_select_fusion.2), channel_id=1, source_target_pairs={{0,16},{16,0},{4,20},{20,4},{8,24},{24,8},{12,28},{28,12},{32,48},... | collective-permute-start | bytes 6291464 | tf_op jit(solution)/shard_map/ppermute | solution.py:23
  72.5 1.9 fusion.1
  74.3 56.9 %collective-permute-done.2 = bf16[2,2,1,128,2048]{4,3,1,2,0:T(8,128)(2,1)} collective-permute-done((bf16[2,2,1,128,2048]{4,3,1,2,0:T(8,128)(2,1)}, bf16[2,2,1,128,2048]{4,3,1,2,0:T(8,128)(2,1)}, u32[]{:S(2)}, u32[]{:S(2)}) %collective-permute-start.2) | collective-permute-done | bytes 2097184 | tf_op jit(solution)/shard_map/ppermute | solution.py:23
  131.2 4.5 %maximum_select_fusion = bf16[2,2,2,1,128,2048]{5,4,2,1,3,0:T(8,128)(2,1)} fusion(bf16[1,2,2,1,128,2048]{5,4,2,1,3,0:T(8,128)(2,1)} %bitcast.13, bf16[1,2,2,1,128,2048]{5,4,2,1,3,0:T(8,128)(2,1)S(1)} %fusion.1, pred[]{:T(512)S(6)} %eq.11), kind=kLoop, calls=%fused_computation | loop fusion | flops 6291456 | bytes 8388609 | tf_op jit(solution)/shard_map/jit(_where)/select_n | solution.py:64
  135.8 2.8 %copy-done.3 = bf16[2,2,2,1,128,2048]{5,4,2,1,3,0:T(8,128)(2,1)S(1)} copy-done((bf16[2,2,2,1,128,2048]{5,4,2,1,3,0:T(8,128)(2,1)S(1)}, bf16[2,2,2,1,128,2048]{5,4,2,1,3,0:T(8,128)(2,1)}, u32[]{:S(2)}) %copy-start.3) | copy-done | bytes 4194328
  139.9 1.3 fusion.7
  141.2 3.2 %copy-done = f32[2,2,2,128,2048]{4,3,2,1,0:T(8,128)} copy-done((f32[2,2,2,128,2048]{4,3,2,1,0:T(8,128)}, f32[2,2,2,128,2048]{4,3,2,1,0:T(8,128)S(1)}, u32[]{:S(2)}) %copy-start) | copy-done | bytes 8388632
  144.7 3.5 %collective-permute-start.3 = (bf16[2,2,128,2048]{3,2,1,0:T(8,128)(2,1)S(1)}, bf16[2,2,128,2048]{3,2,1,0:T(8,128)(2,1)}, u32[]{:S(2)}, u32[]{:S(2)}) collective-permute-start(bf16[2,2,128,2048]{3,2,1,0:T(8,128)(2,1)S(1)} %fusion), channel_id=1, source_target_pairs={{0,4},{4,0},{8,12},{12,8},{16,20},{20,16},{24,28},{28,24},{32,36},... | collective-permute-start | bytes 6291464 | tf_op jit(solution)/shard_map/ppermute | solution.py:23
  148.3 3.9 %collective-permute-done.3 = bf16[2,2,128,2048]{3,2,1,0:T(8,128)(2,1)} collective-permute-done((bf16[2,2,128,2048]{3,2,1,0:T(8,128)(2,1)S(1)}, bf16[2,2,128,2048]{3,2,1,0:T(8,128)(2,1)}, u32[]{:S(2)}, u32[]{:S(2)}) %collective-permute-start.3) | collective-permute-done | bytes 2097184 | tf_op jit(solution)/shard_map/ppermute | solution.py:23
  152.2 3.4 %bitcast_add_fusion = f32[2,2,128,2048]{3,2,1,0:T(8,128)S(1)} fusion(bf16[2,2,128,2048]{3,2,1,0:T(8,128)(2,1)} %collective-permute-done.3, f32[2,2,2,128,2048]{4,3,2,1,0:T(8,128)} %copy-done, s32[]{:T(128)S(6)} %select_n.151), kind=kLoop, calls=%fused_computation.1 | loop fusion | flops 2097152 | bytes 10485764 | tf_op jit(solution)/shard_map/add | solution.py:84
  155.6 1.9 copy-done.1
  157.7 2.1 collective-permute-start.4
  159.8 24.1 %collective-permute-done.4 = bf16[2,128,2048]{2,1,0:T(8,128)(2,1)S(1)} collective-permute-done((bf16[2,128,2048]{2,1,0:T(8,128)(2,1)S(1)}, bf16[2,128,2048]{2,1,0:T(8,128)(2,1)S(1)}, u32[]{:S(2)}, u32[]{:S(2)}) %collective-permute-start.4) | collective-permute-done | bytes 1048608 | tf_op jit(solution)/shard_map/ppermute | solution.py:23
  183.9 1.8 bitcast_add_fusion.1
  185.9 2.6 %collective-permute-start.5 = (bf16[128,2048]{1,0:T(8,128)(2,1)S(1)}, bf16[128,2048]{1,0:T(8,128)(2,1)S(1)}, u32[]{:S(2)}, u32[]{:S(2)}) collective-permute-start(bf16[128,2048]{1,0:T(8,128)(2,1)S(1)} %fusion.11), channel_id=1, source_target_pairs={{0,16},{16,0},{4,20},{20,4},{8,24},{24,8},{12,28},{28,12},{32,48},... | collective-permute-start | bytes 1572872 | tf_op jit(solution)/shard_map/ppermute | solution.py:23
  188.5 13.0 %collective-permute-done.5 = bf16[128,2048]{1,0:T(8,128)(2,1)S(1)} collective-permute-done((bf16[128,2048]{1,0:T(8,128)(2,1)S(1)}, bf16[128,2048]{1,0:T(8,128)(2,1)S(1)}, u32[]{:S(2)}, u32[]{:S(2)}) %collective-permute-start.5) | collective-permute-done | bytes 524320 | tf_op jit(solution)/shard_map/ppermute | solution.py:23
  201.7 10.9 %all_to_all.17 = bf16[4,128,512]{2,1,0:T(8,128)(2,1)S(1)} all-to-all(bf16[4,128,512]{2,1,0:T(8,128)(2,1)S(1)} %bitcast.67), channel_id=1, replica_groups=mesh['fs'=128,'tp'=4] {'tp'}, dimensions={0} | all-to-all | bytes 1048576 | tf_op jit(solution)/shard_map/all_to_all | solution.py:34
  (33 shorter events, 8.4 us)
Async XLA Ops:
  4.4 20.5 %copy-start.5 = (bf16[128,2048]{1,0:T(8,128)(2,1)S(1)}, bf16[128,2048]{1,0:T(8,128)(2,1)}, u32[]{:S(2)}) copy-start(bf16[128,2048]{1,0:T(8,128)(2,1)} %param.4) | copy-start | bytes 1572868
  4.4 131.2 %all-to-all-start = ((bf16[128,16,512]{2,1,0:T(8,128)(2,1)}), bf16[128,16,512]{2,1,0:T(8,128)(2,1)S(1)}, u32[]{:S(2)}, u32[]{:S(2)}) async-start(bf16[128,16,512]{2,1,0:T(8,128)(2,1)} %pad_maximum_fusion), calls=%async_computation | async-start | bytes 4194304 | tf_op jit(solution)/shard_map/all_to_all | solution.py:12
  26.1 4.5 %collective-permute-start = (bf16[1,128,2048]{2,1,0:T(8,128)(2,1)}, bf16[1,128,2048]{2,1,0:T(8,128)(2,1)S(1)}, u32[]{:S(2)}, u32[]{:S(2)}) collective-permute-start(bf16[1,128,2048]{2,1,0:T(8,128)(2,1)} %get-tuple-element.8), channel_id=1, source_target_pairs={{0,4},{4,0},{8,12},{12,8},{16,20},{20,16},{24,28},{28,24},{32,36},... | collective-permute-start | bytes 1572872 | tf_op jit(solution)/shard_map/ppermute | solution.py:23
  31.8 33.8 %collective-permute-start.1 = (bf16[2,1,128,2048]{3,2,1,0:T(8,128)(2,1)}, bf16[2,1,128,2048]{3,2,1,0:T(8,128)(2,1)}, u32[]{:S(2)}, u32[]{:S(2)}) collective-permute-start(bf16[2,1,128,2048]{3,2,1,0:T(8,128)(2,1)} %maximum_select_fusion.4), channel_id=1, source_target_pairs={{0,8},{8,0},{4,12},{12,4},{16,24},{24,16},{20,28},{28,20},{32,40},... | collective-permute-start | bytes 3145736 | tf_op jit(solution)/shard_map/ppermute | solution.py:23
  65.5 6.9 %copy-start.2 = (bf16[1,1,2,128,2048]{4,3,2,1,0:T(8,128)(2,1)S(1)}, bf16[1,1,2,128,2048]{4,3,2,1,0:T(8,128)(2,1)}, u32[]{:S(2)}) copy-start(bf16[1,1,2,128,2048]{4,3,2,1,0:T(8,128)(2,1)} %get-tuple-element.5) | copy-start | bytes 3145732
  68.8 62.4 %collective-permute-start.2 = (bf16[2,2,1,128,2048]{4,3,1,2,0:T(8,128)(2,1)}, bf16[2,2,1,128,2048]{4,3,1,2,0:T(8,128)(2,1)}, u32[]{:S(2)}, u32[]{:S(2)}) collective-permute-start(bf16[2,2,1,128,2048]{4,3,1,2,0:T(8,128)(2,1)} %maximum_select_fusion.2), channel_id=1, source_target_pairs={{0,16},{16,0},{4,20},{20,4},{8,24},{24,8},{12,28},{28,12},{32,48},... | collective-permute-start | bytes 6291464 | tf_op jit(solution)/shard_map/ppermute | solution.py:23
  135.7 2.9 %copy-start.3 = (bf16[2,2,2,1,128,2048]{5,4,2,1,3,0:T(8,128)(2,1)S(1)}, bf16[2,2,2,1,128,2048]{5,4,2,1,3,0:T(8,128)(2,1)}, u32[]{:S(2)}) copy-start(bf16[2,2,2,1,128,2048]{5,4,2,1,3,0:T(8,128)(2,1)} %maximum_select_fusion) | copy-start | bytes 12582916
  135.8 4.1 %copy-start.6 = (bf16[1,2048,256]{2,1,0:T(8,128)(2,1)}, bf16[1,2048,256]{2,1,0:T(8,128)(2,1)S(1)}, u32[]{:S(2)}) copy-start(bf16[1,2048,256]{2,1,0:T(8,128)(2,1)S(1)} %get-tuple-element.4) | copy-start | bytes 3145732
  135.8 4.1 %copy-start.4 = (bf16[1,2048,256]{2,1,0:T(8,128)(2,1)}, bf16[1,2048,256]{2,1,0:T(8,128)(2,1)S(1)}, u32[]{:S(2)}) copy-start(bf16[1,2048,256]{2,1,0:T(8,128)(2,1)S(1)} %get-tuple-element.3) | copy-start | bytes 3145732
  141.2 3.2 %copy-start = (f32[2,2,2,128,2048]{4,3,2,1,0:T(8,128)}, f32[2,2,2,128,2048]{4,3,2,1,0:T(8,128)S(1)}, u32[]{:S(2)}) copy-start(f32[2,2,2,128,2048]{4,3,2,1,0:T(8,128)S(1)} %fusion.7) | copy-start | bytes 25165828
  144.7 7.4 %collective-permute-start.3 = (bf16[2,2,128,2048]{3,2,1,0:T(8,128)(2,1)S(1)}, bf16[2,2,128,2048]{3,2,1,0:T(8,128)(2,1)}, u32[]{:S(2)}, u32[]{:S(2)}) collective-permute-start(bf16[2,2,128,2048]{3,2,1,0:T(8,128)(2,1)S(1)} %fusion), channel_id=1, source_target_pairs={{0,4},{4,0},{8,12},{12,8},{16,20},{20,16},{24,28},{28,24},{32,36},... | collective-permute-start | bytes 6291464 | tf_op jit(solution)/shard_map/ppermute | solution.py:23
  155.6 2.0 copy-start.1
  157.7 26.2 %collective-permute-start.4 = (bf16[2,128,2048]{2,1,0:T(8,128)(2,1)S(1)}, bf16[2,128,2048]{2,1,0:T(8,128)(2,1)S(1)}, u32[]{:S(2)}, u32[]{:S(2)}) collective-permute-start(bf16[2,128,2048]{2,1,0:T(8,128)(2,1)S(1)} %fusion.6), channel_id=1, source_target_pairs={{0,8},{8,0},{4,12},{12,4},{16,24},{24,16},{20,28},{28,20},{32,40},... | collective-permute-start | bytes 3145736 | tf_op jit(solution)/shard_map/ppermute | solution.py:23
  185.9 15.7 %collective-permute-start.5 = (bf16[128,2048]{1,0:T(8,128)(2,1)S(1)}, bf16[128,2048]{1,0:T(8,128)(2,1)S(1)}, u32[]{:S(2)}, u32[]{:S(2)}) collective-permute-start(bf16[128,2048]{1,0:T(8,128)(2,1)S(1)} %fusion.11), channel_id=1, source_target_pairs={{0,16},{16,0},{4,20},{20,4},{8,24},{24,8},{12,28},{28,12},{32,48},... | collective-permute-start | bytes 1572872 | tf_op jit(solution)/shard_map/ppermute | solution.py:23
where the time goes:
time: 215 us; the launch traced here: 213 us
  waiting for transfers between devices  129 us (60%)
  starting transfers between devices  37.9 us (18%)
  other arithmetic  22.7 us (11%)
  blocking collectives  10.9 us (5%)
  local copies, waits for them, and re-layouts  8.89 us (4%)
  matrix products  2.54 us (1%)
    ppermute x6, waiting for transfers between devices, from_partner(): return lax.ppermute(block, axis, route)  129 us
    all_to_all x1, starting transfers between devices, sent_together(): lax.all_to_all(both, axis, split_axis=split_dim, concat_axis=concat_dim,...  20.5 us
    ppermute x6, starting transfers between devices, from_partner(): return lax.ppermute(block, axis, route)  17.4 us
    all_to_all x1, blocking collectives, sum_at_owner(): lax.all_to_all(in_blocks(array, dim, devices), axis, 0, 0, tiled=True)  10.9 us
    select_n x3, other arithmetic, on_device(): jnp.where(lower, jnp.stack([current, partner]), jnp.stack([partner, curre...  8.88 us
    unnamed x16, local copies, waits for them, and re-layouts  7.98 us
    add x2, other arithmetic, on_device(): keep + from_partner(other.astype(jnp.bfloat16), 'fs', bit).astype(other.d...  5.25 us
  transfers between devices with their start and end apart: 7, of which 6 were waited for; matrix products, arithmetic and copies ran while one was open for 6% of the time, Pallas kernels for 0%

commit v1 on v0

v1 whole, which is shorter than its diff:
```python
import jax
import jax.numpy as jnp
import numpy as np
from jax import lax
from jax.sharding import Mesh
from jax.sharding import PartitionSpec as P

SUB = 8
ROOM = 2.0**15
COARSE = 14
SPARE = 8


def power_scale(largest):
    scale = jnp.ones_like(largest)
    factors = []
    for _ in range(SPARE - 1):
        fits = largest * (scale * 2.0**COARSE) < ROOM
        scale = jnp.where(fits, scale * 2.0**COARSE, scale)
        factors.append(jnp.where(fits, 2.0**-COARSE, 1.0))
    last = jnp.ones_like(largest)
    for step in (8, 4, 2):
        fits = largest * (scale * 2.0**step) < ROOM
        scale = jnp.where(fits, scale * 2.0**step, scale)
        last = jnp.where(fits, last * 2.0**-step, last)
    factors.append(last)
    return scale, jnp.stack(factors)


def on_device(tokens, gain, up_master, down_master):
    feat_rows = up_master.shape[0]
    units = up_master.shape[1] // SUB
    x_count = lax.axis_size("x")
    y_count = lax.axis_size("y")
    rows, width = tokens.shape
    up_round = (gain[:, None] * up_master).astype(jnp.bfloat16)
    down_round = down_master.astype(jnp.bfloat16)
    both = jnp.concatenate(
        [up_round.reshape(feat_rows, SUB, units), down_round.reshape(feat_rows, SUB, units)], axis=2
    ).transpose(1, 0, 2)
    both = lax.all_to_all(both, ("x", "c"), 0, 0, tiled=True)
    block = both.reshape(SUB * feat_rows, 2 * units).astype(jnp.float32)

    widened = tokens.astype(jnp.float32)
    normed = (
        widened * lax.rsqrt(jnp.mean(widened * widened, axis=1, keepdims=True) + 1e-06)
    ).astype(jnp.bfloat16)
    held = [normed]
    for ahead in range(1, x_count):
        held.append(lax.ppermute(normed, "x", [((i + ahead) % x_count, i) for i in range(x_count)]))

    scale, factors = power_scale(jnp.max(jnp.abs(block), axis=0))
    packed = jnp.concatenate([block * scale, factors]).astype(jnp.float16)
    spread = lax.all_gather(packed[None], ("z", "c"), axis=0, tiled=True)
    spread = spread.reshape(-1, 2, SUB * feat_rows + SPARE, 2 * units).astype(jnp.float32)
    inverse = jnp.prod(spread[:, :, SUB * feat_rows :], axis=2, keepdims=True)
    weights = (spread[:, :, : SUB * feat_rows] * inverse).astype(jnp.bfloat16)
    core = lax.axis_index("c")
    mine, other = (
        lax.dynamic_index_in_dim(weights, which, 1, keepdims=False).reshape(width, 2 * units)
        for which in (core, 1 - core)
    )
    gathered = jnp.concatenate(held)
    partial_out = 0.0
    for pair in (mine, other):
        pre_units = jnp.dot(gathered, pair[:, :units], preferred_element_type=jnp.float32)
        act_units = jnp.square(jax.nn.relu(pre_units)).astype(jnp.bfloat16)
        partial_out += lax.dot_general(
            act_units, pair[:, units:], (((1,), (1,)), ((), ())), preferred_element_type=jnp.float32
        )
    pieces = partial_out.astype(jnp.bfloat16).reshape(x_count, rows, y_count, width // y_count)
    pieces = jnp.roll(pieces.transpose(0, 2, 1, 3), lax.axis_index("x"), axis=0)
    pieces = pieces.reshape(x_count * y_count, rows, width // y_count)
    pieces = lax.all_to_all(pieces, ("x", "y"), 0, 0, tiled=True)
    mixed = jnp.sum(pieces.astype(jnp.float32), axis=0).astype(jnp.bfloat16)
    return mine[None, :, :units], mine[None, :, units:], mixed


def solution(mesh):
    fine = Mesh(np.reshape(mesh.devices, (16, 4, 2, 4)), ("z", "x", "c", "y"))
    fs = ("z", "x", "c")
    return jax.shard_map(
        on_device,
        mesh=fine,
        in_specs=(P(fs, None), P(fs), P(fs, "y"), P(fs, "y")),
        out_specs=(P(fs, None, "y"), P(fs, None, "y"), P(fs, "y")),
        check_vma=False,
    )
```

time: 215 us -> 136 us (0.63)
  waiting for transfers between devices: 129 us -> 27.8 us
  blocking collectives: 10.9 us -> 46.5 us
  other arithmetic: 22.7 us -> 11 us
  starting transfers between devices: 37.9 us -> 26.3 us
  matrix products: 2.54 us -> 12.2 us
    ppermute x6 -> x3, waiting for transfers between devices: 129 us -> 0.01 us  [on_device(): lax.ppermute(normed, 'x', [((i + ahead) % x_count, i) for i in range(x_co...]
    all_gather x0 -> x1, blocking collectives: none -> 46.5 us  [on_device(): spread = lax.all_gather(packed[None], ('z', 'c'), axis=0, tiled=True)]
    all_to_all x1 -> x2, waiting for transfers between devices: 0.01 us -> 27.8 us  [the longest x1 27.7 us: on_device(): pieces = lax.all_to_all(pieces, ('x', 'y'), 0, 0, tiled=True)]
    all_to_all x1 -> x0, blocking collectives: 10.9 us -> none  [sum_at_owner(): lax.all_to_all(in_blocks(array, dim, devices), axis, 0, 0, tiled=True)]
    dot_general x2, matrix products: 2.54 us -> 12.2 us  [on_device(): lax.dot_general(act_units, pair[:, units:], (((1,), (1,)), ((), ())), pre...]
    select_n x3 -> x1, other arithmetic: 8.88 us -> 0.03 us  [power_scale(): scale = jnp.where(fits, scale * 2.0 ** step, scale)]
    ppermute x6 -> x3, starting transfers between devices: 17.4 us -> 9.47 us  [on_device(): lax.ppermute(normed, 'x', [((i + ahead) % x_count, i) for i in range(x_co...]
    unnamed x16 -> x4, local copies, waits for them, and re-layouts: 7.98 us -> 0.04 us
  transfers between devices with their start and end apart: 7 -> 5, of which waited for: 6 -> 1; matrix products, arithmetic and copies ran while one was open for 6% -> 6% of each run, Pallas kernels for 0% -> 0%
where the time goes in v1:
time: 136 us; the launch traced here: 135 us
  blocking collectives  46.5 us (34%)
  waiting for transfers between devices  27.8 us (20%)
  starting transfers between devices  26.3 us (19%)
  matrix products  12.2 us (9%)
  other arithmetic  11 us (8%)
  local copies, waits for them, and re-layouts  10.4 us (8%)
    all_gather x1, blocking collectives, on_device(): spread = lax.all_gather(packed[None], ('z', 'c'), axis=0, tiled=True)  46.5 us
    all_to_all x1, waiting for transfers between devices, on_device(): pieces = lax.all_to_all(pieces, ('x', 'y'), 0, 0, tiled=True)  27.7 us
    dot_general x2, matrix products, on_device(): lax.dot_general(act_units, pair[:, units:], (((1,), (1,)), ((), ())), pre...  12.2 us
    all_to_all x1, starting transfers between devices, on_device(): both = lax.all_to_all(both, ('x', 'c'), 0, 0, tiled=True)  10.1 us
    ppermute x3, starting transfers between devices, on_device(): lax.ppermute(normed, 'x', [((i + ahead) % x_count, i) for i in range(x_co...  9.47 us
    all_to_all x1, starting transfers between devices, on_device(): pieces = lax.all_to_all(pieces, ('x', 'y'), 0, 0, tiled=True)  6.71 us
    reshape x2, local copies, waits for them, and re-layouts, on_device(): partial_out.astype(jnp.bfloat16)  6.53 us
  transfers between devices with their start and end apart: 5, of which 1 were waited for; matrix products, arithmetic and copies ran while one was open for 6% of the time, Pallas kernels for 0%

profile of v1, /device:TPU:1, one launch (start us, length us, event | category | flops | bytes accessed | tf_op | source)
XLA Modules:
  0.0 135.1 jit_solution(17065079970946331733)
XLA Ops:
  0.6 1.0 multiply_convert_fusion
  1.7 0.9 convert_element_type.56
  2.7 0.7 copy.10
  3.4 10.1 %all-to-all-start = ((bf16[8,16,512]{2,1,0:T(8,128)(2,1)}), bf16[8,16,512]{2,1,0:T(8,128)(2,1)S(1)}, u32[]{:S(2)}, u32[]{:S(2)}) async-start(bf16[8,16,512]{2,1,0:T(8,128)(2,1)} %copy.10), calls=%async_computation | async-start | bytes 262144 | tf_op jit(solution)/shard_map/all_to_all | solution.py:41
  13.5 1.2 fusion.7
  14.7 0.2 fusion.8
  14.9 4.5 %collective-permute-start = (bf16[128,2048]{1,0:T(8,128)(2,1)S(1)}, bf16[128,2048]{1,0:T(8,128)(2,1)S(1)}, u32[]{:S(2)}, u32[]{:S(2)}) collective-permute-start(bf16[128,2048]{1,0:T(8,128)(2,1)S(1)} %fusion.8), channel_id=1, source_target_pairs={{8,0},{16,8},{24,16},{0,24},{9,1},{17,9},{25,17},{1,25},{10,2},{18... | collective-permute-start | bytes 1572872 | tf_op jit(solution)/shard_map/ppermute | solution.py:50
  19.4 2.5 %collective-permute-start.1 = (bf16[128,2048]{1,0:T(8,128)(2,1)S(1)}, bf16[128,2048]{1,0:T(8,128)(2,1)}, u32[]{:S(2)}, u32[]{:S(2)}) collective-permute-start(bf16[128,2048]{1,0:T(8,128)(2,1)S(1)} %fusion.8), channel_id=1, source_target_pairs={{16,0},{24,8},{0,16},{8,24},{17,1},{25,9},{1,17},{9,25},{18,2},{26... | collective-permute-start | bytes 1572872 | tf_op jit(solution)/shard_map/ppermute | solution.py:50
  21.9 2.5 %collective-permute-start.2 = (bf16[128,2048]{1,0:T(8,128)(2,1)S(1)}, bf16[128,2048]{1,0:T(8,128)(2,1)}, u32[]{:S(2)}, u32[]{:S(2)}) collective-permute-start(bf16[128,2048]{1,0:T(8,128)(2,1)S(1)} %fusion.8), channel_id=1, source_target_pairs={{24,0},{0,8},{8,16},{16,24},{25,1},{1,9},{9,17},{17,25},{26,2},{2,... | collective-permute-start | bytes 1572872 | tf_op jit(solution)/shard_map/ppermute | solution.py:50
  24.6 0.1 concatenate.49
  24.7 46.5 %all-gather.1 = f16[32,136,512]{2,1,0:T(8,128)(2,1)S(1)} all-gather(f16[1,136,512]{2,1,0:T(8,128)(2,1)S(1)} %concatenate.49), channel_id=1, replica_groups=mesh['z'=16,'x'=4,'c'=2,'y'=4] {'z','c'}, dimensions={0}, use_global_device_ids=true | all-gather | bytes 4595712 | tf_op jit(solution)/shard_map/all_gather | solution.py:54
  71.2 1.3 bitcast_convert_fusion
  72.5 0.2 slice_reduce_fusion
  72.7 1.4 %fusion = bf16[16,2,128,512]{3,2,1,0:T(8,128)(2,1)S(1)} fusion(f32[16,2,136,512]{3,2,1,0:T(8,128)S(1)} %bitcast_convert_fusion, f32[16,2,512]{2,1,0:T(2,128)S(1)} %slice_reduce_fusion), kind=kLoop, calls=%fused_computation.1 | loop fusion | flops 4194304 | bytes 12648448 | tf_op jit(solution)/shard_map/convert_element_type | solution.py:57
  74.1 1.6 %constant_dynamic-slice_fusion = (bf16[16,1,128,512]{3,2,1,0:T(8,128)(2,1)}, bf16[16,1,128,512]{3,2,1,0:T(8,128)(2,1)S(1)}) fusion(bf16[16,2,128,512]{3,2,1,0:T(8,128)(2,1)S(1)} %fusion, s32[]{:T(128)S(6)} %select_n.618, s32[]{:T(128)S(6)} %select_n.617), kind=kLoop, calls=%fused_computation.103 | loop fusion | bytes 8388616 | tf_op jit(solution)/shard_map/jit(dynamic_index_in_dim)/dynamic_slice | solution.py:60
  75.8 5.4 %fusion.6 = f32[512,2048]{1,0:T(8,128)} fusion(bf16[2048,512]{1,0:T(8,128)(2,1)S(1)} %bitcast.41, bf16[128,2048]{1,0:T(8,128)(2,1)} %collective-permute-done.2, bf16[128,2048]{1,0:T(8,128)(2,1)} %collective-permute-done.1, bf16[128,2048]{1,0:T(8,128)(2,1)S(1)} %collective-permute-done, bf16[128,2048]{1,0:T(8,128)(2,1)S(1)} %fusion.8), kind=kOutput, calls=%fused_computation.16 | convolution fusion | flops 1082523648 | bytes 8388608 | tf_op jit(solution)/shard_map/dot_general | solution.py:68
  81.2 6.8 %add_convert_fusion = bf16[512,2048]{1,0:T(8,128)(2,1)} fusion(f32[512,2048]{1,0:T(8,128)} %fusion.6, bf16[2048,512]{1,0:T(8,128)(2,1)} %bitcast.45, bf16[128,2048]{1,0:T(8,128)(2,1)} %collective-permute-done.2, bf16[128,2048]{1,0:T(8,128)(2,1)} %collective-permute-done.1, bf16[128,2048]{1,0:T(8,128)(2,1)S(1)} %collective-permute-done, ...), kind=kOutput, calls=%fused_computation.4 | convolution fusion | flops 1084620800 | bytes 10485760 | tf_op jit(solution)/shard_map/dot_general | solution.py:68
  88.0 4.5 %reshape.384 = bf16[4,128,4,512]{3,2,1,0:T(4,128)(2,1)} reshape(bf16[512,2048]{1,0:T(8,128)(2,1)} %add_convert_fusion) | data formatting | bytes 4194304 | tf_op jit(solution)/shard_map/reshape | solution.py:71
  92.5 2.0 %copy.15 = bf16[4,128,4,512]{3,1,2,0:T(8,128)(2,1)S(1)} copy(bf16[4,128,4,512]{3,2,1,0:T(4,128)(2,1)} %reshape.384) | data formatting | bytes 4194304 | tf_op jit(solution)/shard_map/reshape | solution.py:71
  94.6 2.1 %fusion.1 = bf16[4,4,128,512]{3,2,1,0:T(8,128)(2,1)} fusion(s32[]{:T(128)S(6)} %select_n.620, bf16[4,4,128,512]{3,2,1,0:T(8,128)(2,1)S(1)} %bitcast.44), kind=kLoop, calls=%fused_computation.5 | loop fusion | flops 1048576 | bytes 4194308 | tf_op jit(solution)/shard_map/jit(_roll_dynamic)/concatenate | solution.py:72
  96.6 6.7 %all-to-all-start.1 = ((bf16[16,128,512]{2,1,0:T(8,128)(2,1)}), bf16[16,128,512]{2,1,0:T(8,128)(2,1)}, u32[]{:S(2)}, u32[]{:S(2)}) async-start(bf16[16,128,512]{2,1,0:T(8,128)(2,1)} %bitcast.43), calls=%async_computation.1 | async-start | bytes 4194304 | tf_op jit(solution)/shard_map/all_to_all | solution.py:74
  103.3 1.5 %slice_bitcast_fusion = (bf16[1,2048,256]{2,1,0:T(8,128)(2,1)}, bf16[1,2048,256]{2,1,0:T(8,128)(2,1)}) fusion(bf16[2048,512]{1,0:T(8,128)(2,1)S(1)} %bitcast.42), kind=kLoop, calls=%fused_computation.22 | loop fusion | bytes 4194304 | tf_op jit(solution)/shard_map/broadcast_in_dim | solution.py:76
  104.8 27.7 %all-to-all-done.1 = bf16[16,128,512]{2,1,0:T(8,128)(2,1)} async-done(((bf16[16,128,512]{2,1,0:T(8,128)(2,1)}), bf16[16,128,512]{2,1,0:T(8,128)(2,1)}, u32[]{:S(2)}, u32[]{:S(2)}) %all-to-all-start.1) | async-done | bytes 2097184 | tf_op jit(solution)/shard_map/all_to_all | solution.py:74
  132.5 2.6 %reduce_sum.22 = bf16[128,512]{1,0:T(8,128)(2,1)} reduce(bf16[16,128,512]{2,1,0:T(8,128)(2,1)} %all-to-all-done.1, bf16[]{:T(256)} %constant.76.clone.1), dimensions={0}, to_apply=%region_3.4 | reduce | flops 983040 | bytes 2228226 | tf_op jit(solution)/shard_map/reduce_sum | solution.py:75
  (15 shorter events, 0.2 us)
Async XLA Ops:
  0.6 14.1 %copy-start = (bf16[128,2048]{1,0:T(8,128)(2,1)S(1)}, bf16[128,2048]{1,0:T(8,128)(2,1)}, u32[]{:S(2)}) copy-start(bf16[128,2048]{1,0:T(8,128)(2,1)} %param.4) | copy-start | bytes 1572868
  3.4 21.0 %all-to-all-start = ((bf16[8,16,512]{2,1,0:T(8,128)(2,1)}), bf16[8,16,512]{2,1,0:T(8,128)(2,1)S(1)}, u32[]{:S(2)}, u32[]{:S(2)}) async-start(bf16[8,16,512]{2,1,0:T(8,128)(2,1)} %copy.10), calls=%async_computation | async-start | bytes 262144 | tf_op jit(solution)/shard_map/all_to_all | solution.py:41
  14.9 60.9 %collective-permute-start = (bf16[128,2048]{1,0:T(8,128)(2,1)S(1)}, bf16[128,2048]{1,0:T(8,128)(2,1)S(1)}, u32[]{:S(2)}, u32[]{:S(2)}) collective-permute-start(bf16[128,2048]{1,0:T(8,128)(2,1)S(1)} %fusion.8), channel_id=1, source_target_pairs={{8,0},{16,8},{24,16},{0,24},{9,1},{17,9},{25,17},{1,25},{10,2},{18... | collective-permute-start | bytes 1572872 | tf_op jit(solution)/shard_map/ppermute | solution.py:50
  19.4 56.4 %collective-permute-start.1 = (bf16[128,2048]{1,0:T(8,128)(2,1)S(1)}, bf16[128,2048]{1,0:T(8,128)(2,1)}, u32[]{:S(2)}, u32[]{:S(2)}) collective-permute-start(bf16[128,2048]{1,0:T(8,128)(2,1)S(1)} %fusion.8), channel_id=1, source_target_pairs={{16,0},{24,8},{0,16},{8,24},{17,1},{25,9},{1,17},{9,25},{18,2},{26... | collective-permute-start | bytes 1572872 | tf_op jit(solution)/shard_map/ppermute | solution.py:50
  21.9 53.9 %collective-permute-start.2 = (bf16[128,2048]{1,0:T(8,128)(2,1)S(1)}, bf16[128,2048]{1,0:T(8,128)(2,1)}, u32[]{:S(2)}, u32[]{:S(2)}) collective-permute-start(bf16[128,2048]{1,0:T(8,128)(2,1)S(1)} %fusion.8), channel_id=1, source_target_pairs={{24,0},{0,8},{8,16},{16,24},{25,1},{1,9},{9,17},{17,25},{26,2},{2,... | collective-permute-start | bytes 1572872 | tf_op jit(solution)/shard_map/ppermute | solution.py:50
  96.6 35.9 %all-to-all-start.1 = ((bf16[16,128,512]{2,1,0:T(8,128)(2,1)}), bf16[16,128,512]{2,1,0:T(8,128)(2,1)}, u32[]{:S(2)}, u32[]{:S(2)}) async-start(bf16[16,128,512]{2,1,0:T(8,128)(2,1)} %bitcast.43), calls=%async_computation.1 | async-start | bytes 4194304 | tf_op jit(solution)/shard_map/all_to_all | solution.py:74

commit v2 on v1

v2 whole, which is shorter than its diff:
```python
import functools

import jax
import jax.numpy as jnp
import numpy as np
from jax import lax
from jax.experimental import pallas as pl
from jax.experimental.pallas import tpu as pltpu
from jax.sharding import Mesh
from jax.sharding import PartitionSpec as P

SUB = 8
ROOM = 2.0**15
COARSE = 14
SPARE = 8


def power_scale(largest):
    scale = jnp.ones_like(largest)
    factors = []
    for _ in range(SPARE - 1):
        fits = largest * (scale * 2.0**COARSE) < ROOM
        scale = jnp.where(fits, scale * 2.0**COARSE, scale)
        factors.append(jnp.where(fits, 2.0**-COARSE, 1.0))
    last = jnp.ones_like(largest)
    for step in (8, 4, 2):
        fits = largest * (scale * 2.0**step) < ROOM
        scale = jnp.where(fits, scale * 2.0**step, scale)
        last = jnp.where(fits, last * 2.0**-step, last)
    factors.append(last)
    return scale, jnp.stack(factors)


def apply_kernel(units, core_ref, tokens, spread, up_out, down_out, pieces, up, down, hidden, sems):
    core = core_ref[0]
    x_count, rows, width = tokens.shape
    y_count = pieces.shape[0] // x_count
    feats = spread.shape[1] - SPARE
    part = width // y_count

    def unpack(z, carry):
        for half in range(2):
            packed = spread[2 * z + (core if half == 0 else 1 - core)].astype(jnp.float32)
            inverse = packed[feats : feats + 1]
            for k in range(1, SPARE):
                inverse = inverse * packed[feats + k : feats + k + 1]
            values = (packed[:feats] * inverse).astype(jnp.bfloat16)
            at = pl.ds(pl.multiple_of(z * feats, feats), feats)
            up[at, half * units : (half + 1) * units] = values[:, :units]
            down[at, half * units : (half + 1) * units] = values[:, units:]
        return carry

    lax.fori_loop(0, width // feats, unpack, 0)
    hidden[...] = jnp.zeros_like(hidden)

    for k in range(y_count):
        cols = slice(k * part, (k + 1) * part)
        hidden[...] += jnp.dot(
            tokens[:, :, cols].reshape(x_count * rows, part),
            up[cols, :],
            preferred_element_type=jnp.float32,
        )
    copies = [
        pltpu.make_async_copy(source.at[:, :units], target, sems.at[i])
        for i, (source, target) in enumerate(((up, up_out), (down, down_out)))
    ]
    for copy in copies:
        copy.start()
    act = jnp.square(jnp.maximum(hidden[...], 0.0)).astype(jnp.bfloat16)
    for y in range(y_count):
        out = lax.dot_general(
            act,
            down[y * part : (y + 1) * part, :],
            (((1,), (1,)), ((), ())),
            preferred_element_type=jnp.float32,
        ).astype(jnp.bfloat16)
        for x in range(x_count):
            pieces[x * y_count + y] = out[x * rows : (x + 1) * rows]
    for copy in copies:
        copy.wait()


def apply(core, tokens, spread, y_count):
    x_count, rows, width = tokens.shape
    units = spread.shape[2] // 2
    weight = jax.ShapeDtypeStruct((width, units), jnp.bfloat16)
    vmem = pl.BlockSpec(memory_space=pltpu.VMEM)
    anywhere = pl.BlockSpec(memory_space=pl.ANY)
    return pl.pallas_call(
        functools.partial(apply_kernel, units),
        out_shape=(
            weight,
            weight,
            jax.ShapeDtypeStruct((x_count * y_count, rows, width // y_count), jnp.bfloat16),
        ),
        in_specs=[pl.BlockSpec(memory_space=pltpu.SMEM), vmem, vmem],
        out_specs=(anywhere, anywhere, vmem),
        scratch_shapes=[
            pltpu.VMEM((width, 2 * units), jnp.bfloat16),
            pltpu.VMEM((width, 2 * units), jnp.bfloat16),
            pltpu.VMEM((x_count * rows, 2 * units), jnp.float32),
            pltpu.SemaphoreType.DMA((2,)),
        ],
        cost_estimate=pl.CostEstimate(
            flops=8 * x_count * rows * width * units, bytes_accessed=16 << 20, transcendentals=0
        ),
        compiler_params=pltpu.CompilerParams(vmem_limit_bytes=40 << 20),
    )(core, tokens, spread)


def on_device(tokens, gain, up_master, down_master):
    feat_rows = up_master.shape[0]
    units = up_master.shape[1] // SUB
    x_count = lax.axis_size("x")
    y_count = lax.axis_size("y")
    up_round = (gain[:, None] * up_master).astype(jnp.bfloat16)
    down_round = down_master.astype(jnp.bfloat16)
    both = jnp.concatenate(
        [up_round.reshape(feat_rows, SUB, units), down_round.reshape(feat_rows, SUB, units)], axis=2
    ).transpose(1, 0, 2)
    both = lax.all_to_all(both, ("x", "c"), 0, 0, tiled=True)

    widened = tokens.astype(jnp.float32)
    normed = (
        widened * lax.rsqrt(jnp.mean(widened * widened, axis=1, keepdims=True) + 1e-06)
    ).astype(jnp.bfloat16)
    copies = jnp.broadcast_to(normed[None], (x_count, *normed.shape))
    both, copies = lax.optimization_barrier((both, copies))
    gathered = lax.all_to_all(copies, "x", 0, 0, tiled=True)

    block = both.reshape(SUB * feat_rows, 2 * units).astype(jnp.float32)
    scale, factors = power_scale(jnp.max(jnp.abs(block), axis=0))
    packed = jnp.concatenate([block * scale, factors]).astype(jnp.float16)
    spread = lax.all_gather(packed[None], ("z", "c"), axis=0, tiled=True)
    core = lax.axis_index("c").astype(jnp.int32)[None]
    up_own, down_own, pieces = apply(core, gathered, spread.astype(jnp.bfloat16), y_count)
    pieces = lax.all_to_all(pieces, ("x", "y"), 0, 0, tiled=True)
    mixed = jnp.sum(pieces.astype(jnp.float32), axis=0).astype(jnp.bfloat16)
    return up_own[None], down_own[None], mixed


def solution(mesh):
    fine = Mesh(np.reshape(mesh.devices, (16, 4, 2, 4)), ("z", "x", "c", "y"))
    fs = ("z", "x", "c")
    return jax.shard_map(
        on_device,
        mesh=fine,
        in_specs=(P(fs, None), P(fs), P(fs, "y"), P(fs, "y")),
        out_specs=(P(fs, None, "y"), P(fs, None, "y"), P(fs, "y")),
        check_vma=False,
    )
```

time: 136 us -> 115 us (0.85)
  blocking collectives: 46.5 us -> 81.1 us
  waiting for transfers between devices: 27.8 us -> 2.82 us
  starting transfers between devices: 26.3 us -> 13.7 us
  matrix products: 12.2 us -> 0 us
  local copies, waits for them, and re-layouts: 10.4 us -> 4.01 us
  Pallas kernels: 0 us -> 3.41 us
  other arithmetic: 11 us -> 9.05 us
    all_to_all x0 -> x1, blocking collectives: none -> 34.2 us  [on_device(): pieces = lax.all_to_all(pieces, ('x', 'y'), 0, 0, tiled=True)]
    all_to_all x1, waiting for transfers between devices: 27.7 us -> 0.01 us  [on_device(): gathered = lax.all_to_all(copies, 'x', 0, 0, tiled=True)]
    dot_general x2 -> x0, matrix products: 12.2 us -> none  [on_device(): lax.dot_general(act_units, pair[:, units:], (((1,), (1,)), ((), ())), pre...]
    ppermute x3 -> x0, starting transfers between devices: 9.47 us -> none  [on_device(): lax.ppermute(normed, 'x', [((i + ahead) % x_count, i) for i in range(x_co...]
    reshape x2 -> x1, local copies, waits for them, and re-layouts: 6.53 us -> 0.01 us  [on_device(): down_round.reshape(feat_rows, SUB, units)]
    pallas_call x0 -> x1, Pallas kernels: none -> 3.41 us  [apply(): pl.pallas_call(functools.partial(apply_kernel, units), out_shape=(weight,...]
    all_to_all x1, starting transfers between devices: 6.71 us -> 3.62 us  [on_device(): gathered = lax.all_to_all(copies, 'x', 0, 0, tiled=True)]
    all_to_all x1, waiting for transfers between devices: 0.01 us -> 2.82 us  [on_device(): both = lax.all_to_all(both, ('x', 'c'), 0, 0, tiled=True)]
  transfers between devices with their start and end apart: 5 -> 2, of which waited for: 1 -> 1; matrix products, arithmetic and copies ran while one was open for 6% -> 5% of each run, Pallas kernels for 0% -> 0%
where the time goes in v2:
time: 115 us
  blocking collectives  81.1 us (71%)
  starting transfers between devices  13.7 us (12%)
  other arithmetic  9.05 us (8%)
  local copies, waits for them, and re-layouts  4.01 us (3%)
  Pallas kernels  3.41 us (3%)
  waiting for transfers between devices  2.82 us (2%)
    all_gather x1, blocking collectives, on_device(): spread = lax.all_gather(packed[None], ('z', 'c'), axis=0, tiled=True)  47 us
    all_to_all x1, blocking collectives, on_device(): pieces = lax.all_to_all(pieces, ('x', 'y'), 0, 0, tiled=True)  34.2 us
    all_to_all x1, starting transfers between devices, on_device(): both = lax.all_to_all(both, ('x', 'c'), 0, 0, tiled=True)  10.1 us
    all_to_all x1, starting transfers between devices, on_device(): gathered = lax.all_to_all(copies, 'x', 0, 0, tiled=True)  3.62 us
    pallas_call x1, Pallas kernels, apply(): pl.pallas_call(functools.partial(apply_kernel, units), out_shape=(weight,...  3.41 us
    convert_element_type x1, other arithmetic, on_device(): spread.astype(jnp.bfloat16)  2.92 us
    all_to_all x1, waiting for transfers between devices, on_device(): both = lax.all_to_all(both, ('x', 'c'), 0, 0, tiled=True)  2.82 us
  transfers between devices with their start and end apart: 2, of which 1 were waited for; matrix products, arithmetic and copies ran while one was open for 5% of the time, Pallas kernels for 0%

profile of v2, /device:TPU:1, one launch (start us, length us, event | category | flops | bytes accessed | tf_op | source)
XLA Modules:
  0.0 114.8 jit_solution(3099415591612966908)
XLA Ops:
  0.6 0.9 convert_element_type.41
  1.5 1.0 multiply_convert_fusion
  2.5 0.7 maximum_bitcast_fusion
  3.2 10.1 %all-to-all-start = ((bf16[8,16,512]{2,1,0:T(8,128)(2,1)}), bf16[8,16,512]{2,1,0:T(8,128)(2,1)S(1)}, u32[]{:S(2)}, u32[]{:S(2)}) async-start(bf16[8,16,512]{2,1,0:T(8,128)(2,1)} %maximum_bitcast_fusion), calls=%async_computation | async-start | bytes 262144 | tf_op jit(solution)/shard_map/all_to_all | solution.py:121
  13.3 1.2 %fusion = f32[128]{0:T(128)S(1)} fusion(bf16[128,2048]{1,0:T(8,128)(2,1)} %param.4), kind=kLoop, calls=%fused_computation.2 | loop fusion | flops 786304 | bytes 524800 | tf_op jit(solution)/shard_map/reduce_sum | solution.py:125
  14.6 1.2 %fusion.1 = bf16[128,2048]{1,0:T(8,128)(2,1)S(1)} fusion(bf16[128,2048]{1,0:T(8,128)(2,1)} %param.4, f32[128]{0:T(128)S(1)} %add_rsqrt_fusion), kind=kLoop, calls=%fused_computation.3 | loop fusion | flops 786432 | bytes 1049088 | tf_op jit(solution)/shard_map/convert_element_type | solution.py:126
  15.8 2.8 %all-to-all-done = bf16[8,16,512]{2,1,0:T(8,128)(2,1)S(1)} async-done(((bf16[8,16,512]{2,1,0:T(8,128)(2,1)}), bf16[8,16,512]{2,1,0:T(8,128)(2,1)S(1)}, u32[]{:S(2)}, u32[]{:S(2)}) %all-to-all-start) | async-done | bytes 131104 | tf_op jit(solution)/shard_map/all_to_all | solution.py:121
  18.6 1.6 %broadcast_in_dim.38 = bf16[4,128,2048]{2,1,0:T(8,128)(2,1)} broadcast(bf16[128,2048]{1,0:T(8,128)(2,1)S(1)} %fusion.1), dimensions={1,2} | broadcast | bytes 2621440 | tf_op jit(solution)/shard_map/broadcast_in_dim | solution.py:127
  20.4 3.6 %all-to-all-start.1 = ((bf16[4,128,2048]{2,1,0:T(8,128)(2,1)}), bf16[4,128,2048]{2,1,0:T(8,128)(2,1)S(1)}, u32[]{:S(2)}, u32[]{:S(2)}) async-start(bf16[4,128,2048]{2,1,0:T(8,128)(2,1)} %broadcast_in_dim.38), calls=%async_computation.1 | async-start | bytes 4194304 | tf_op jit(solution)/shard_map/all_to_all | solution.py:129
  24.0 0.1 concatenate.42
  24.2 47.0 %all-gather.1 = f16[32,136,512]{2,1,0:T(8,128)(2,1)S(1)} all-gather(f16[1,136,512]{2,1,0:T(8,128)(2,1)S(1)} %concatenate.42), channel_id=1, replica_groups=mesh['z'=16,'x'=4,'c'=2,'y'=4] {'z','c'}, dimensions={0}, use_global_device_ids=true | all-gather | bytes 4595712 | tf_op jit(solution)/shard_map/all_gather | solution.py:134
  71.1 2.9 %convert_element_type.47.spread = bf16[32,136,512]{2,1,0:T(8,128)(2,1)} convert(f16[32,136,512]{2,1,0:T(8,128)(2,1)S(1)} %all-gather.1) | non-fusion elementwise | flops 2228224 | bytes 8912896 | tf_op jit(solution)/shard_map/convert_element_type | solution.py:136
  74.0 0.0 all-to-all-done.1.tokens
  74.0 0.0 copy-start
  74.0 2.3 %copy-done = bf16[32,136,512]{2,1,0:T(8,128)(2,1)S(1)} copy-done((bf16[32,136,512]{2,1,0:T(8,128)(2,1)S(1)}, bf16[32,136,512]{2,1,0:T(8,128)(2,1)}, u32[]{:S(2)}) %copy-start) | copy-done | bytes 4456472
  76.3 3.4 %shard_map.67 = (bf16[2048,256]{1,0:T(8,128)(2,1)}, bf16[2048,256]{1,0:T(8,128)(2,1)}, bf16[16,128,512]{2,1,0:T(8,128)(2,1)S(1)}) custom-call(s32[1]{0:T(128)} %bitcast.core_ref, bf16[4,128,2048]{2,1,0:T(8,128)(2,1)S(1)} %all-to-all-done.1.tokens, bf16[32,136,512]{2,1,0:T(8,128)(2,1)S(1)} %copy-done), custom_call_target="tpu_custom_call" | custom-call | flops 2147483648 | bytes 16777216 | tf_op jit(solution)/shard_map/pallas_call | solution.py:89
  79.7 34.2 %all_to_all.15 = bf16[16,128,512]{2,1,0:T(8,128)(2,1)S(1)} all-to-all(bf16[16,128,512]{2,1,0:T(8,128)(2,1)S(1)} %get-tuple-element.12), channel_id=1, replica_groups=mesh['z'=16,'x'=4,'c'=2,'y'=4] {'x','y'}, dimensions={0} | all-to-all | bytes 4194304 | tf_op jit(solution)/shard_map/all_to_all | solution.py:137
  113.9 1.0 reduce_sum.22
  (7 shorter events, 0.2 us)
Async XLA Ops:
  3.2 15.4 %all-to-all-start = ((bf16[8,16,512]{2,1,0:T(8,128)(2,1)}), bf16[8,16,512]{2,1,0:T(8,128)(2,1)S(1)}, u32[]{:S(2)}, u32[]{:S(2)}) async-start(bf16[8,16,512]{2,1,0:T(8,128)(2,1)} %maximum_bitcast_fusion), calls=%async_computation | async-start | bytes 262144 | tf_op jit(solution)/shard_map/all_to_all | solution.py:121
  20.4 53.7 %all-to-all-start.1 = ((bf16[4,128,2048]{2,1,0:T(8,128)(2,1)}), bf16[4,128,2048]{2,1,0:T(8,128)(2,1)S(1)}, u32[]{:S(2)}, u32[]{:S(2)}) async-start(bf16[4,128,2048]{2,1,0:T(8,128)(2,1)} %broadcast_in_dim.38), calls=%async_computation.1 | async-start | bytes 4194304 | tf_op jit(solution)/shard_map/all_to_all | solution.py:129
  74.0 2.3 %copy-start = (bf16[32,136,512]{2,1,0:T(8,128)(2,1)S(1)}, bf16[32,136,512]{2,1,0:T(8,128)(2,1)}, u32[]{:S(2)}) copy-start(bf16[32,136,512]{2,1,0:T(8,128)(2,1)} %convert_element_type.47.spread) | copy-start | bytes 13369348

commit v3 on v2

--- a/solution.py
+++ b/solution.py
@@ -31,20 +31,64 @@
     return scale, jnp.stack(factors)
 
 
-def apply_kernel(units, core_ref, tokens, spread, up_out, down_out, pieces, up, down, hidden, sems):
+def fold_kernel(gain, up, down, out):
+    members, _, columns = out.shape
+    units = columns // 2
+    for m in range(members):
+        at = slice(m * units, (m + 1) * units)
+        out[m, :, :units] = (gain[...] * up[:, at]).astype(jnp.bfloat16)
+        out[m, :, units:] = down[:, at].astype(jnp.bfloat16)
+
+
+def fold(gain, up, down):
+    rows, columns = up.shape
+    return pl.pallas_call(
+        fold_kernel,
+        out_shape=jax.ShapeDtypeStruct((SUB, rows, 2 * columns // SUB), jnp.bfloat16),
+        cost_estimate=pl.CostEstimate(
+            flops=2 * up.size, bytes_accessed=12 * up.size, transcendentals=0
+        ),
+        compiler_params=pltpu.CompilerParams(vmem_limit_bytes=4 << 20),
+    )(gain, up, down)
+
+
+def norm_kernel(tokens, out, normed, sems):
+    widened = tokens[...].astype(jnp.float32)
+    mean = jnp.mean(widened * widened, axis=1, keepdims=True)
+    normed[...] = (widened * lax.rsqrt(mean + 1e-06)).astype(jnp.bfloat16)
+    copies = [pltpu.make_async_copy(normed, out.at[x], sems.at[x]) for x in range(out.shape[0])]
+    for copy in copies:
+        copy.start()
+    for copy in copies:
+        copy.wait()
+
+
+def norm_copies(tokens, count):
+    return pl.pallas_call(
+        norm_kernel,
+        out_shape=jax.ShapeDtypeStruct((count, *tokens.shape), jnp.bfloat16),
+        out_specs=pl.BlockSpec(memory_space=pltpu.HBM),
+        scratch_shapes=[
+            pltpu.VMEM(tokens.shape, jnp.bfloat16),
+            pltpu.SemaphoreType.DMA((count,)),
+        ],
+        cost_estimate=pl.CostEstimate(
+            flops=2_000_000_000, bytes_accessed=10 * tokens.size, transcendentals=tokens.shape[0]
+        ),
+        compiler_params=pltpu.CompilerParams(vmem_limit_bytes=8 << 20),
+    )(tokens)
+
+
+def apply_kernel(units, core_ref, tokens, weights, up_out, down_out, pieces, up, down, hidden, sems):
     core = core_ref[0]
     x_count, rows, width = tokens.shape
     y_count = pieces.shape[0] // x_count
-    feats = spread.shape[1] - SPARE
+    feats = weights.shape[1]
     part = width // y_count
 
     def unpack(z, carry):
         for half in range(2):
-            packed = spread[2 * z + (core if half == 0 else 1 - core)].astype(jnp.float32)
-            inverse = packed[feats : feats + 1]
-            for k in range(1, SPARE):
-                inverse = inverse * packed[feats + k : feats + k + 1]
-            values = (packed[:feats] * inverse).astype(jnp.bfloat16)
+            values = weights[2 * z + (core if half == 0 else 1 - core)]
             at = pl.ds(pl.multiple_of(z * feats, feats), feats)
             up[at, half * units : (half + 1) * units] = values[:, :units]
             down[at, half * units : (half + 1) * units] = values[:, units:]
@@ -80,9 +124,9 @@
         copy.wait()
 
 
-def apply(core, tokens, spread, y_count):
+def apply(core, tokens, weights, y_count):
     x_count, rows, width = tokens.shape
-    units = spread.shape[2] // 2
+    units = weights.shape[2] // 2
     weight = jax.ShapeDtypeStruct((width, units), jnp.bfloat16)
     vmem = pl.BlockSpec(memory_space=pltpu.VMEM)
     anywhere = pl.BlockSpec(memory_space=pl.ANY)
@@ -104,36 +148,30 @@
         cost_estimate=pl.CostEstimate(
             flops=8 * x_count * rows * width * units, bytes_accessed=16 << 20, transcendentals=0
         ),
-        compiler_params=pltpu.CompilerParams(vmem_limit_bytes=40 << 20),
-    )(core, tokens, spread)
+        compiler_params=pltpu.CompilerParams(vmem_limit_bytes=20 << 20),
+    )(core, tokens, weights)
 
 
 def on_device(tokens, gain, up_master, down_master):
     feat_rows = up_master.shape[0]
     units = up_master.shape[1] // SUB
+    feats = SUB * feat_rows
     x_count = lax.axis_size("x")
     y_count = lax.axis_size("y")
-    up_round = (gain[:, None] * up_master).astype(jnp.bfloat16)
-    down_round = down_master.astype(jnp.bfloat16)
-    both = jnp.concatenate(
-        [up_round.reshape(feat_rows, SUB, units), down_round.reshape(feat_rows, SUB, units)], axis=2
-    ).transpose(1, 0, 2)
+    both = fold(gain[:, None], up_master, down_master)
     both = lax.all_to_all(both, ("x", "c"), 0, 0, tiled=True)
+    gathered = lax.all_to_all(norm_copies(tokens, x_count), "x", 0, 0, tiled=True)
 
-    widened = tokens.astype(jnp.float32)
-    normed = (
-        widened * lax.rsqrt(jnp.mean(widened * widened, axis=1, keepdims=True) + 1e-06)
-    ).astype(jnp.bfloat16)
-    copies = jnp.broadcast_to(normed[None], (x_count, *normed.shape))
-    both, copies = lax.optimization_barrier((both, copies))
-    gathered = lax.all_to_all(copies, "x", 0, 0, tiled=True)
-
-    block = both.reshape(SUB * feat_rows, 2 * units).astype(jnp.float32)
+    block = both.reshape(feats, 2 * units).astype(jnp.float32)
     scale, factors = power_scale(jnp.max(jnp.abs(block), axis=0))
     packed = jnp.concatenate([block * scale, factors]).astype(jnp.float16)
     spread = lax.all_gather(packed[None], ("z", "c"), axis=0, tiled=True)
+    spread, gathered = lax.optimization_barrier((spread, gathered))
+    tail = lax.optimization_barrier(spread[:, feats:])
+    inverse = jnp.prod(tail.astype(jnp.float32), axis=1, keepdims=True)
+    weights = (spread[:, :feats].astype(jnp.float32) * inverse).astype(jnp.bfloat16)
     core = lax.axis_index("c").astype(jnp.int32)[None]
-    up_own, down_own, pieces = apply(core, gathered, spread.astype(jnp.bfloat16), y_count)
+    up_own, down_own, pieces = apply(core, gathered, weights, y_count)
     pieces = lax.all_to_all(pieces, ("x", "y"), 0, 0, tiled=True)
     mixed = jnp.sum(pieces.astype(jnp.float32), axis=0).astype(jnp.bfloat16)
     return up_own[None], down_own[None], mixed

time: 115 us -> 114 us (level)
  other arithmetic: 9.05 us -> 4.61 us
  local copies, waits for them, and re-layouts: 4.01 us -> 6.04 us
  blocking collectives: 81.1 us -> 82.6 us
    convert_element_type x4 -> x1, other arithmetic: 6.01 us -> 3.29 us  [on_device(): (spread[:, :feats].astype(jnp.float32) * inverse).astype(jnp.bfloat16)]
    unnamed x2 -> x8, local copies, waits for them, and re-layouts: 2.26 us -> 4.2 us
    all_gather x1, blocking collectives: 47 us -> 48.5 us  [on_device(): spread = lax.all_gather(packed[None], ('z', 'c'), axis=0, tiled=True)]
    reduce_sum x1 -> x0, other arithmetic: 1.23 us -> none  [on_device(): jnp.mean(widened * widened, axis=1, keepdims=True) + 1e-06]
  transfers between devices with their start and end apart: 2 -> 2, of which waited for: 1 -> 1; matrix products, arithmetic and copies ran while one was open for 5% -> 0% of each run, Pallas kernels for 0% -> 0%
where the time goes in v3:
time: 114 us
  blocking collectives  82.6 us (72%)
  starting transfers between devices  13.7 us (12%)
  local copies, waits for them, and re-layouts  6.04 us (5%)
  other arithmetic  4.61 us (4%)
  Pallas kernels  3.81 us (3%)
  waiting for transfers between devices  2.47 us (2%)
    all_gather x1, blocking collectives, on_device(): spread = lax.all_gather(packed[None], ('z', 'c'), axis=0, tiled=True)  48.5 us
    all_to_all x1, blocking collectives, on_device(): pieces = lax.all_to_all(pieces, ('x', 'y'), 0, 0, tiled=True)  34 us
    all_to_all x1, starting transfers between devices, on_device(): both = lax.all_to_all(both, ('x', 'c'), 0, 0, tiled=True)  10.1 us
    unnamed x8, local copies, waits for them, and re-layouts  4.2 us
    all_to_all x1, starting transfers between devices, on_device(): lax.all_to_all(norm_copies(tokens, x_count), 'x', 0, 0, tiled=True)  3.61 us
    convert_element_type x1, other arithmetic, on_device(): (spread[:, :feats].astype(jnp.float32) * inverse).astype(jnp.bfloat16)  3.29 us
    pallas_call x1, Pallas kernels, apply(): pl.pallas_call(functools.partial(apply_kernel, units), out_shape=(weight,...  2.69 us
    all_to_all x1, waiting for transfers between devices, on_device(): both = lax.all_to_all(both, ('x', 'c'), 0, 0, tiled=True)  2.47 us
  transfers between devices with their start and end apart: 2, of which 1 were waited for; matrix products, arithmetic and copies ran while one was open for 0% of the time, Pallas kernels for 0%

profile of v3, /device:TPU:1, one launch (start us, length us, event | category | flops | bytes accessed | tf_op | source)
XLA Modules:
  0.0 113.9 jit_solution(1902398482479833821)
XLA Ops:
  0.6 0.7 copy.8.gain
  1.4 0.0 copy-start.1
  1.4 0.9 copy-done.1
  2.3 0.0 copy-start.2
  2.3 0.9 copy-done.2
  3.2 0.7 shard_map.67
  3.9 10.1 %all-to-all-start = ((bf16[8,16,512]{2,1,0:T(8,128)(2,1)}), bf16[8,16,512]{2,1,0:T(8,128)(2,1)S(1)}, u32[]{:S(2)}, u32[]{:S(2)}) async-start(bf16[8,16,512]{2,1,0:T(8,128)(2,1)} %shard_map.67), calls=%async_computation | async-start | bytes 262144 | tf_op jit(solution)/shard_map/all_to_all | solution.py:162
  14.0 0.0 copy-start.3
  14.0 1.0 copy-done.3
  15.1 0.4 shard_map.68
  15.5 0.0 copy-start
  15.5 1.4 %copy-done = bf16[4,128,2048]{2,1,0:T(8,128)(2,1)} copy-done((bf16[4,128,2048]{2,1,0:T(8,128)(2,1)}, bf16[4,128,2048]{2,1,0:T(8,128)(2,1)S(1)}, u32[]{:S(2)}) %copy-start) | copy-done | bytes 2097176
  16.8 2.5 %all-to-all-done = bf16[8,16,512]{2,1,0:T(8,128)(2,1)S(1)} async-done(((bf16[8,16,512]{2,1,0:T(8,128)(2,1)}), bf16[8,16,512]{2,1,0:T(8,128)(2,1)S(1)}, u32[]{:S(2)}, u32[]{:S(2)}) %all-to-all-start) | async-done | bytes 131104 | tf_op jit(solution)/shard_map/all_to_all | solution.py:162
  19.3 3.6 %all-to-all-start.1 = ((bf16[4,128,2048]{2,1,0:T(8,128)(2,1)}), bf16[4,128,2048]{2,1,0:T(8,128)(2,1)S(1)}, u32[]{:S(2)}, u32[]{:S(2)}) async-start(bf16[4,128,2048]{2,1,0:T(8,128)(2,1)} %copy-done), calls=%async_computation.1 | async-start | bytes 4194304 | tf_op jit(solution)/shard_map/all_to_all | solution.py:163
  23.1 0.1 concatenate.38
  23.2 48.5 %all-gather.1 = f16[32,136,512]{2,1,0:T(8,128)(2,1)} all-gather(f16[1,136,512]{2,1,0:T(8,128)(2,1)S(1)} %concatenate.38), channel_id=1, replica_groups=mesh['z'=16,'x'=4,'c'=2,'y'=4] {'z','c'}, dimensions={0}, use_global_device_ids=true | all-gather | bytes 4595712 | tf_op jit(solution)/shard_map/all_gather | solution.py:168
  71.7 0.0 all-to-all-done.1.tokens
  71.7 1.0 slice.7
  72.7 0.2 convert_reduce_fusion
  72.9 3.3 %multiply_convert_fusion.weights = bf16[32,128,512]{2,1,0:T(8,128)(2,1)S(1)} fusion(f32[32,512]{1,0:T(8,128)S(1)} %convert_reduce_fusion, f16[32,136,512]{2,1,0:T(8,128)(2,1)} %all-gather.1), kind=kLoop, calls=%fused_computation | loop fusion | flops 6291456 | bytes 8454144 | tf_op jit(solution)/shard_map/convert_element_type | solution.py:172
  76.2 2.7 %shard_map.69 = (bf16[2048,256]{1,0:T(8,128)(2,1)}, bf16[2048,256]{1,0:T(8,128)(2,1)}, bf16[16,128,512]{2,1,0:T(8,128)(2,1)S(1)}) custom-call(s32[1]{0:T(128)} %bitcast.core_ref, bf16[4,128,2048]{2,1,0:T(8,128)(2,1)S(1)} %all-to-all-done.1.tokens, bf16[32,128,512]{2,1,0:T(8,128)(2,1)S(1)} %multiply_convert_fusion.weights), custom_call_target="tpu_custom_call" | custom-call | flops 2147483648 | bytes 16777216 | tf_op jit(solution)/shard_map/pallas_call | solution.py:133
  78.9 34.0 %all_to_all.15 = bf16[16,128,512]{2,1,0:T(8,128)(2,1)S(1)} all-to-all(bf16[16,128,512]{2,1,0:T(8,128)(2,1)S(1)} %get-tuple-element.12), channel_id=1, replica_groups=mesh['z'=16,'x'=4,'c'=2,'y'=4] {'x','y'}, dimensions={0} | all-to-all | bytes 4194304 | tf_op jit(solution)/shard_map/all_to_all | solution.py:175
  112.9 1.0 reduce_sum.12
  (5 shorter events, 0.2 us)
Async XLA Ops:
  1.4 0.9 copy-start.1
  2.3 0.9 copy-start.2
  3.9 15.4 %all-to-all-start = ((bf16[8,16,512]{2,1,0:T(8,128)(2,1)}), bf16[8,16,512]{2,1,0:T(8,128)(2,1)S(1)}, u32[]{:S(2)}, u32[]{:S(2)}) async-start(bf16[8,16,512]{2,1,0:T(8,128)(2,1)} %shard_map.67), calls=%async_computation | async-start | bytes 262144 | tf_op jit(solution)/shard_map/all_to_all | solution.py:162
  14.0 1.0 copy-start.3
  15.5 1.4 %copy-start = (bf16[4,128,2048]{2,1,0:T(8,128)(2,1)}, bf16[4,128,2048]{2,1,0:T(8,128)(2,1)S(1)}, u32[]{:S(2)}) copy-start(bf16[4,128,2048]{2,1,0:T(8,128)(2,1)S(1)} %shard_map.68) | copy-start | bytes 6291460
  19.3 52.4 %all-to-all-start.1 = ((bf16[4,128,2048]{2,1,0:T(8,128)(2,1)}), bf16[4,128,2048]{2,1,0:T(8,128)(2,1)S(1)}, u32[]{:S(2)}, u32[]{:S(2)}) async-start(bf16[4,128,2048]{2,1,0:T(8,128)(2,1)} %copy-done), calls=%async_computation.1 | async-start | bytes 4194304 | tf_op jit(solution)/shard_map/all_to_all | solution.py:163

commit v4 on v3

--- a/solution.py
+++ b/solution.py
@@ -31,12 +31,25 @@
     return scale, jnp.stack(factors)
 
 
-def fold_kernel(gain, up, down, out):
-    members, _, columns = out.shape
+def fold_kernel(gain_in, up_in, down_in, out, gain, up, down, sems):
+    loads = [
+        pltpu.make_async_copy(source, target, sems.at[i])
+        for i, (source, target) in enumerate(
+            ((gain_in, gain), (up_in, up), (down_in, down))
+        )
+    ]
+    for load in loads:
+        load.start()
+    for load in loads:
+        load.wait()
+    members, rows, columns = out.shape
     units = columns // 2
+    square = (rows, rows)
+    here = lax.broadcasted_iota(jnp.int32, square, 0) == lax.broadcasted_iota(jnp.int32, square, 1)
+    spread = jnp.sum(jnp.where(here, jnp.broadcast_to(gain[...], square), 0.0), axis=1, keepdims=True)
     for m in range(members):
         at = slice(m * units, (m + 1) * units)
-        out[m, :, :units] = (gain[...] * up[:, at]).astype(jnp.bfloat16)
+        out[m, :, :units] = (spread * up[:, at]).astype(jnp.bfloat16)
         out[m, :, units:] = down[:, at].astype(jnp.bfloat16)
 
 
@@ -45,10 +58,16 @@
     return pl.pallas_call(
         fold_kernel,
         out_shape=jax.ShapeDtypeStruct((SUB, rows, 2 * columns // SUB), jnp.bfloat16),
+        in_specs=[pl.BlockSpec(memory_space=pl.ANY)] * 3,
+        scratch_shapes=[
+            pltpu.VMEM(gain.shape, jnp.float32),
+            pltpu.VMEM(up.shape, jnp.float32),
+            pltpu.VMEM(up.shape, jnp.float32),
+            pltpu.SemaphoreType.DMA((3,)),
+        ],
         cost_estimate=pl.CostEstimate(
             flops=2 * up.size, bytes_accessed=12 * up.size, transcendentals=0
         ),
-        compiler_params=pltpu.CompilerParams(vmem_limit_bytes=4 << 20),
     )(gain, up, down)
 
 
@@ -75,7 +94,6 @@
         cost_estimate=pl.CostEstimate(
             flops=2_000_000_000, bytes_accessed=10 * tokens.size, transcendentals=tokens.shape[0]
         ),
-        compiler_params=pltpu.CompilerParams(vmem_limit_bytes=8 << 20),
     )(tokens)
 
 
@@ -83,12 +101,16 @@
     core = core_ref[0]
     x_count, rows, width = tokens.shape
     y_count = pieces.shape[0] // x_count
-    feats = weights.shape[1]
+    feats = weights.shape[1] - SPARE
     part = width // y_count
 
     def unpack(z, carry):
         for half in range(2):
-            values = weights[2 * z + (core if half == 0 else 1 - core)]
+            packed = weights[2 * z + (core if half == 0 else 1 - core)]
+            inverse = packed[feats : feats + 1]
+            for k in range(1, SPARE):
+                inverse = inverse * packed[feats + k : feats + k + 1]
+            values = (packed[:feats] * inverse).astype(jnp.bfloat16)
             at = pl.ds(pl.multiple_of(z * feats, feats), feats)
             up[at, half * units : (half + 1) * units] = values[:, :units]
             down[at, half * units : (half + 1) * units] = values[:, units:]
@@ -119,7 +141,8 @@
             preferred_element_type=jnp.float32,
         ).astype(jnp.bfloat16)
         for x in range(x_count):
-            pieces[x * y_count + y] = out[x * rows : (x + 1) * rows]
+            place = jnp.where(core == 0, x * y_count + y, y * x_count + x)
+            pieces[place] = out[x * rows : (x + 1) * rows]
     for copy in copies:
         copy.wait()
 
@@ -148,8 +171,21 @@
         cost_estimate=pl.CostEstimate(
             flops=8 * x_count * rows * width * units, bytes_accessed=16 << 20, transcendentals=0
         ),
-        compiler_params=pltpu.CompilerParams(vmem_limit_bytes=20 << 20),
+        compiler_params=pltpu.CompilerParams(vmem_limit_bytes=24 << 20),
     )(core, tokens, weights)
+
+
+def crossed_groups(x_count, y_count):
+    def at(x, c, y):
+        return (x * 2 + c) * y_count + y
+
+    def along_x(c):
+        return [[at(x, c, y) for x in range(x_count)] for y in range(y_count)]
+
+    def along_y(c):
+        return [[at(x, c, y) for y in range(y_count)] for x in range(x_count)]
+
+    return along_x(0) + along_y(1), along_y(0) + along_x(1)
 
 
 def on_device(tokens, gain, up_master, down_master):
@@ -158,7 +194,7 @@
     feats = SUB * feat_rows
     x_count = lax.axis_size("x")
     y_count = lax.axis_size("y")
-    both = fold(gain[:, None], up_master, down_master)
+    both = fold(gain[None], up_master, down_master)
     both = lax.all_to_all(both, ("x", "c"), 0, 0, tiled=True)
     gathered = lax.all_to_all(norm_copies(tokens, x_count), "x", 0, 0, tiled=True)
 
@@ -167,14 +203,15 @@
     packed = jnp.concatenate([block * scale, factors]).astype(jnp.float16)
     spread = lax.all_gather(packed[None], ("z", "c"), axis=0, tiled=True)
     spread, gathered = lax.optimization_barrier((spread, gathered))
-    tail = lax.optimization_barrier(spread[:, feats:])
-    inverse = jnp.prod(tail.astype(jnp.float32), axis=1, keepdims=True)
-    weights = (spread[:, :feats].astype(jnp.float32) * inverse).astype(jnp.bfloat16)
     core = lax.axis_index("c").astype(jnp.int32)[None]
-    up_own, down_own, pieces = apply(core, gathered, weights, y_count)
-    pieces = lax.all_to_all(pieces, ("x", "y"), 0, 0, tiled=True)
-    mixed = jnp.sum(pieces.astype(jnp.float32), axis=0).astype(jnp.bfloat16)
-    return up_own[None], down_own[None], mixed
+    up_own, down_own, pieces = apply(core, gathered, spread.astype(jnp.float32), y_count)
+    for groups in crossed_groups(x_count, y_count):
+        pieces = lax.all_to_all(
+            pieces, ("x", "c", "y"), 0, 0, tiled=True, axis_index_groups=groups
+        )
+        pieces = pieces.reshape(len(groups[0]), -1, *pieces.shape[1:])
+        pieces = jnp.sum(pieces.astype(jnp.float32), axis=0).astype(jnp.bfloat16)
+    return up_own[None], down_own[None], pieces[0]
 
 
 def solution(mesh):

time: 114 us -> 110 us (0.965)
  local copies, waits for them, and re-layouts: 6.04 us -> 0.11 us
  Pallas kernels: 3.81 us -> 8.07 us
  blocking collectives: 82.6 us -> 79.4 us
    unnamed x8 -> x0, local copies, waits for them, and re-layouts: 4.2 us -> none
    all_to_all x1 -> x2, blocking collectives: 34 us -> 30.9 us  [on_device(): lax.all_to_all(pieces, ('x', 'c', 'y'), 0, 0, tiled=True, axis_index_grou...]
    pallas_call x1, Pallas kernels: 0.38 us -> 2.61 us  [norm_copies(): pl.pallas_call(norm_kernel, out_shape=jax.ShapeDtypeStruct((count, *token...]
  transfers between devices with their start and end apart: 2 -> 2, of which waited for: 1 -> 1; matrix products, arithmetic and copies ran while one was open for 0% -> 0% of each run, Pallas kernels for 0% -> 2%
where the time goes in v4:
time: 110 us
  blocking collectives  79.4 us (72%)
  starting transfers between devices  13.7 us (12%)
  Pallas kernels  8.07 us (7%)
  other arithmetic  5.03 us (5%)
  waiting for transfers between devices  2.65 us (2%)
    all_gather x1, blocking collectives, on_device(): spread = lax.all_gather(packed[None], ('z', 'c'), axis=0, tiled=True)  48.5 us
    all_to_all x2, blocking collectives, on_device(): lax.all_to_all(pieces, ('x', 'c', 'y'), 0, 0, tiled=True, axis_index_grou...  30.9 us
    all_to_all x1, starting transfers between devices, on_device(): both = lax.all_to_all(both, ('x', 'c'), 0, 0, tiled=True)  10.1 us
    pallas_call x1, Pallas kernels, apply(): pl.pallas_call(functools.partial(apply_kernel, units), out_shape=(weight,...  3.71 us
    all_to_all x1, starting transfers between devices, on_device(): lax.all_to_all(norm_copies(tokens, x_count), 'x', 0, 0, tiled=True)  3.61 us
    convert_element_type x1, other arithmetic, on_device(): spread.astype(jnp.float32)  3.53 us
    all_to_all x1, waiting for transfers between devices, on_device(): both = lax.all_to_all(both, ('x', 'c'), 0, 0, tiled=True)  2.65 us
    pallas_call x1, Pallas kernels, norm_copies(): pl.pallas_call(norm_kernel, out_shape=jax.ShapeDtypeStruct((count, *token...  2.61 us
  transfers between devices with their start and end apart: 2, of which 1 were waited for; matrix products, arithmetic and copies ran while one was open for 0% of the time, Pallas kernels for 2%

profile of v4, /device:TPU:1, one launch (start us, length us, event | category | flops | bytes accessed | tf_op | source)
XLA Modules:
  0.0 109.6 jit_solution(13974500033946382342)
XLA Ops:
  0.6 1.8 %shard_map.67 = bf16[8,16,512]{2,1,0:T(8,128)(2,1)} custom-call(f32[1,16]{1,0:T(1,128)} %bitcast.31, f32[16,2048]{1,0:T(8,128)} %up_in.1, f32[16,2048]{1,0:T(8,128)} %down_in.1), custom_call_target="tpu_custom_call" | custom-call | flops 65536 | bytes 393216 | tf_op jit(solution)/shard_map/pallas_call | solution.py:58
  2.4 10.1 %all-to-all-start = ((bf16[8,16,512]{2,1,0:T(8,128)(2,1)}), bf16[8,16,512]{2,1,0:T(8,128)(2,1)S(1)}, u32[]{:S(2)}, u32[]{:S(2)}) async-start(bf16[8,16,512]{2,1,0:T(8,128)(2,1)} %shard_map.67), calls=%async_computation | async-start | bytes 262144 | tf_op jit(solution)/shard_map/all_to_all | solution.py:198
  12.5 2.6 %shard_map.68 = bf16[4,128,2048]{2,1,0:T(8,128)(2,1)} custom-call(bf16[128,2048]{1,0:T(8,128)(2,1)} %tokens.1), custom_call_target="tpu_custom_call" | custom-call | flops 2000000000 | bytes 2621440 | tf_op jit(solution)/shard_map/pallas_call | solution.py:86
  15.1 2.6 %all-to-all-done = bf16[8,16,512]{2,1,0:T(8,128)(2,1)S(1)} async-done(((bf16[8,16,512]{2,1,0:T(8,128)(2,1)}), bf16[8,16,512]{2,1,0:T(8,128)(2,1)S(1)}, u32[]{:S(2)}, u32[]{:S(2)}) %all-to-all-start) | async-done | bytes 131104 | tf_op jit(solution)/shard_map/all_to_all | solution.py:198
  17.8 3.6 %all-to-all-start.1 = ((bf16[4,128,2048]{2,1,0:T(8,128)(2,1)}), bf16[4,128,2048]{2,1,0:T(8,128)(2,1)S(1)}, u32[]{:S(2)}, u32[]{:S(2)}) async-start(bf16[4,128,2048]{2,1,0:T(8,128)(2,1)} %shard_map.68), calls=%async_computation.1 | async-start | bytes 4194304 | tf_op jit(solution)/shard_map/all_to_all | solution.py:199
  21.6 0.1 concatenate.38
  21.7 48.5 %all-gather.1 = f16[32,136,512]{2,1,0:T(8,128)(2,1)} all-gather(f16[1,136,512]{2,1,0:T(8,128)(2,1)S(1)} %concatenate.38), channel_id=1, replica_groups=mesh['z'=16,'x'=4,'c'=2,'y'=4] {'z','c'}, dimensions={0}, use_global_device_ids=true | all-gather | bytes 4595712 | tf_op jit(solution)/shard_map/all_gather | solution.py:204
  70.2 0.0 all-to-all-done.1.tokens
  70.2 3.5 %convert_element_type.33.weights = f32[32,136,512]{2,1,0:T(8,128)S(1)} convert(f16[32,136,512]{2,1,0:T(8,128)(2,1)} %all-gather.1) | non-fusion elementwise | flops 2228224 | bytes 13369344 | tf_op jit(solution)/shard_map/convert_element_type | solution.py:207
  73.7 3.7 %shard_map.69 = (bf16[2048,256]{1,0:T(8,128)(2,1)}, bf16[2048,256]{1,0:T(8,128)(2,1)}, bf16[16,128,512]{2,1,0:T(8,128)(2,1)S(1)}) custom-call(s32[1]{0:T(128)} %bitcast.core_ref, bf16[4,128,2048]{2,1,0:T(8,128)(2,1)S(1)} %all-to-all-done.1.tokens, f32[32,136,512]{2,1,0:T(8,128)S(1)} %convert_element_type.33.weights), custom_call_target="tpu_custom_call" | custom-call | flops 2147483648 | bytes 16777216 | tf_op jit(solution)/shard_map/pallas_call | solution.py:156
  77.5 19.4 %all_to_all.20 = bf16[16,128,512]{2,1,0:T(8,128)(2,1)S(1)} all-to-all(bf16[16,128,512]{2,1,0:T(8,128)(2,1)S(1)} %get-tuple-element.12), channel_id=1, replica_groups={{0,8,16,24},{1,9,17,25},{2,10,18,26},{3,11,19,27},{4,5,6,7},{12,13,14,1..., dimensions={0} | all-to-all | bytes 4194304 | tf_op jit(solution)/shard_map/all_to_all | solution.py:209
  96.9 0.6 reduce_sum.24
  97.5 11.4 %all_to_all.21 = bf16[4,128,512]{2,1,0:T(8,128)(2,1)S(1)} all-to-all(bf16[4,128,512]{2,1,0:T(8,128)(2,1)S(1)} %reduce_sum.24), channel_id=1, replica_groups={{0,1,2,3},{8,9,10,11},{16,17,18,19},{24,25,26,27},{4,12,20,28},{5,13,21..., dimensions={0} | all-to-all | bytes 1048576 | tf_op jit(solution)/shard_map/all_to_all | solution.py:209
  108.9 0.7 reduce_sum.25
  (5 shorter events, 0.2 us)
Async XLA Ops:
  2.4 15.4 %all-to-all-start = ((bf16[8,16,512]{2,1,0:T(8,128)(2,1)}), bf16[8,16,512]{2,1,0:T(8,128)(2,1)S(1)}, u32[]{:S(2)}, u32[]{:S(2)}) async-start(bf16[8,16,512]{2,1,0:T(8,128)(2,1)} %shard_map.67), calls=%async_computation | async-start | bytes 262144 | tf_op jit(solution)/shard_map/all_to_all | solution.py:198
  17.8 52.4 %all-to-all-start.1 = ((bf16[4,128,2048]{2,1,0:T(8,128)(2,1)}), bf16[4,128,2048]{2,1,0:T(8,128)(2,1)S(1)}, u32[]{:S(2)}, u32[]{:S(2)}) async-start(bf16[4,128,2048]{2,1,0:T(8,128)(2,1)} %shard_map.68), calls=%async_computation.1 | async-start | bytes 4194304 | tf_op jit(solution)/shard_map/all_to_all | solution.py:199

commit v5 on v4

--- a/solution.py
+++ b/solution.py
@@ -10,54 +10,56 @@
 from jax.sharding import PartitionSpec as P
 
 SUB = 8
+LANES = 128
 ROOM = 2.0**15
-COARSE = 14
-SPARE = 8
+FACTORS = 4
+REACH = 28
+GRANT = 47 << 20
 
 
 def power_scale(largest):
     scale = jnp.ones_like(largest)
     factors = []
-    for _ in range(SPARE - 1):
-        fits = largest * (scale * 2.0**COARSE) < ROOM
-        scale = jnp.where(fits, scale * 2.0**COARSE, scale)
-        factors.append(jnp.where(fits, 2.0**-COARSE, 1.0))
-    last = jnp.ones_like(largest)
-    for step in (8, 4, 2):
+    for _ in range(FACTORS - 1):
+        fits = largest * (scale * 2.0**REACH) < ROOM
+        scale = jnp.where(fits, scale * 2.0**REACH, scale)
+        factors.append(jnp.where(fits, ROOM * 2.0**-REACH, ROOM))
+    last = jnp.full_like(largest, ROOM)
+    for step in (16, 8, 4):
         fits = largest * (scale * 2.0**step) < ROOM
         scale = jnp.where(fits, scale * 2.0**step, scale)
         last = jnp.where(fits, last * 2.0**-step, last)
     factors.append(last)
-    return scale, jnp.stack(factors)
+    return scale, jnp.stack(factors, axis=1)
 
 
 def fold_kernel(gain_in, up_in, down_in, out, gain, up, down, sems):
     loads = [
         pltpu.make_async_copy(source, target, sems.at[i])
-        for i, (source, target) in enumerate(
-            ((gain_in, gain), (up_in, up), (down_in, down))
-        )
+        for i, (source, target) in enumerate(((gain_in, gain), (up_in, up), (down_in, down)))
     ]
     for load in loads:
         load.start()
     for load in loads:
         load.wait()
-    members, rows, columns = out.shape
-    units = columns // 2
+    chips, double, rows, _ = out.shape
+    slabs = double // 2
     square = (rows, rows)
     here = lax.broadcasted_iota(jnp.int32, square, 0) == lax.broadcasted_iota(jnp.int32, square, 1)
     spread = jnp.sum(jnp.where(here, jnp.broadcast_to(gain[...], square), 0.0), axis=1, keepdims=True)
-    for m in range(members):
-        at = slice(m * units, (m + 1) * units)
-        out[m, :, :units] = (spread * up[:, at]).astype(jnp.bfloat16)
-        out[m, :, units:] = down[:, at].astype(jnp.bfloat16)
-
-
-def fold(gain, up, down):
+    for x in range(chips):
+        for slab in range(slabs):
+            first = (x * slabs + slab) * LANES
+            out[x, slab] = (spread * up[:, first : first + LANES]).astype(jnp.bfloat16)
+            out[x, slabs + slab] = down[:, first : first + LANES].astype(jnp.bfloat16)
+
+
+def fold(gain, up, down, chips):
     rows, columns = up.shape
+    slabs = columns // chips // LANES
     return pl.pallas_call(
         fold_kernel,
-        out_shape=jax.ShapeDtypeStruct((SUB, rows, 2 * columns // SUB), jnp.bfloat16),
+        out_shape=jax.ShapeDtypeStruct((chips, 2 * slabs, rows, LANES), jnp.bfloat16),
         in_specs=[pl.BlockSpec(memory_space=pl.ANY)] * 3,
         scratch_shapes=[
             pltpu.VMEM(gain.shape, jnp.float32),
@@ -97,28 +99,52 @@
     )(tokens)
 
 
-def apply_kernel(units, core_ref, tokens, weights, up_out, down_out, pieces, up, down, hidden, sems):
+def apply_kernel(
+    feat_rows, core_ref, tokens, weights, up_out, down_out, pieces, held, up, down, hidden, load_sems, sems
+):
     core = core_ref[0]
     x_count, rows, width = tokens.shape
     y_count = pieces.shape[0] // x_count
-    feats = weights.shape[1] - SPARE
     part = width // y_count
+    units = up_out.shape[1]
+    z_count = held.shape[0]
+    slab_rows = x_count * feat_rows
+    unit_slabs = units // LANES
+    slabs = 2 * unit_slabs
+    last = 2 * slabs * slab_rows
+
+    def load(z):
+        return pltpu.make_async_copy(weights.at[z], held.at[z], load_sems.at[z])
+
+    for z in range(z_count):
+        load(z).start()
 
     def unpack(z, carry):
-        for half in range(2):
-            packed = weights[2 * z + (core if half == 0 else 1 - core)]
-            inverse = packed[feats : feats + 1]
-            for k in range(1, SPARE):
-                inverse = inverse * packed[feats + k : feats + k + 1]
-            values = (packed[:feats] * inverse).astype(jnp.bfloat16)
-            at = pl.ds(pl.multiple_of(z * feats, feats), feats)
-            up[at, half * units : (half + 1) * units] = values[:, :units]
-            down[at, half * units : (half + 1) * units] = values[:, units:]
+        load(z).wait()
+        for source in range(2):
+            for matrix, target in enumerate((up, down)):
+                first = last + matrix * FACTORS
+                factors = held[z, source, first : first + FACTORS].astype(jnp.float32)
+                inverse = factors[0:1] * ROOM**-FACTORS
+                for k in range(1, FACTORS):
+                    inverse = inverse * factors[k : k + 1]
+                for half in range(2):
+                    member = core if half == 0 else 1 - core
+                    for j in range(unit_slabs):
+                        slab = matrix * slabs + member * unit_slabs + j
+                        start = pl.multiple_of(slab * slab_rows, slab_rows)
+                        packed = held[z, source, pl.ds(start, slab_rows)].astype(jnp.float32)
+                        values = (packed * inverse).astype(jnp.bfloat16)
+                        column = half * units + j * LANES
+                        for x in range(x_count):
+                            row = ((z * x_count + x) * 2 + source) * feat_rows
+                            target[pl.ds(pl.multiple_of(row, feat_rows), feat_rows), column : column + LANES] = (
+                                values[x * feat_rows : (x + 1) * feat_rows]
+                            )
         return carry
 
-    lax.fori_loop(0, width // feats, unpack, 0)
+    lax.fori_loop(0, z_count, unpack, 0)
     hidden[...] = jnp.zeros_like(hidden)
-
     for k in range(y_count):
         cols = slice(k * part, (k + 1) * part)
         hidden[...] += jnp.dot(
@@ -147,31 +173,32 @@
         copy.wait()
 
 
-def apply(core, tokens, weights, y_count):
+def apply(core, tokens, weights, units, feat_rows, y_count):
     x_count, rows, width = tokens.shape
-    units = weights.shape[2] // 2
     weight = jax.ShapeDtypeStruct((width, units), jnp.bfloat16)
     vmem = pl.BlockSpec(memory_space=pltpu.VMEM)
     anywhere = pl.BlockSpec(memory_space=pl.ANY)
     return pl.pallas_call(
-        functools.partial(apply_kernel, units),
+        functools.partial(apply_kernel, feat_rows),
         out_shape=(
             weight,
             weight,
             jax.ShapeDtypeStruct((x_count * y_count, rows, width // y_count), jnp.bfloat16),
         ),
-        in_specs=[pl.BlockSpec(memory_space=pltpu.SMEM), vmem, vmem],
+        in_specs=[pl.BlockSpec(memory_space=pltpu.SMEM), vmem, anywhere],
         out_specs=(anywhere, anywhere, vmem),
         scratch_shapes=[
+            pltpu.VMEM(weights.shape, jnp.bfloat16),
             pltpu.VMEM((width, 2 * units), jnp.bfloat16),
             pltpu.VMEM((width, 2 * units), jnp.bfloat16),
             pltpu.VMEM((x_count * rows, 2 * units), jnp.float32),
+            pltpu.SemaphoreType.DMA((weights.shape[0],)),
             pltpu.SemaphoreType.DMA((2,)),
         ],
         cost_estimate=pl.CostEstimate(
             flops=8 * x_count * rows * width * units, bytes_accessed=16 << 20, transcendentals=0
         ),
-        compiler_params=pltpu.CompilerParams(vmem_limit_bytes=24 << 20),
+        compiler_params=pltpu.CompilerParams(vmem_limit_bytes=GRANT),
     )(core, tokens, weights)
 
 
@@ -191,20 +218,20 @@
 def on_device(tokens, gain, up_master, down_master):
     feat_rows = up_master.shape[0]
     units = up_master.shape[1] // SUB
-    feats = SUB * feat_rows
     x_count = lax.axis_size("x")
     y_count = lax.axis_size("y")
-    both = fold(gain[None], up_master, down_master)
-    both = lax.all_to_all(both, ("x", "c"), 0, 0, tiled=True)
+    both = fold(gain[None], up_master, down_master, x_count)
+    both = lax.all_to_all(both, "x", 0, 0, tiled=True)
     gathered = lax.all_to_all(norm_copies(tokens, x_count), "x", 0, 0, tiled=True)
 
-    block = both.reshape(feats, 2 * units).astype(jnp.float32)
-    scale, factors = power_scale(jnp.max(jnp.abs(block), axis=0))
-    packed = jnp.concatenate([block * scale, factors]).astype(jnp.float16)
+    block = both.astype(jnp.float32).reshape(x_count, 2, -1, feat_rows, LANES)
+    scale, factors = power_scale(jnp.max(jnp.abs(block), axis=(0, 2, 3)))
+    packed = (block * scale[None, :, None, None]).transpose(1, 2, 0, 3, 4).reshape(-1, LANES)
+    packed = jnp.concatenate([packed, factors.reshape(-1, LANES)]).astype(jnp.float16)
     spread = lax.all_gather(packed[None], ("z", "c"), axis=0, tiled=True)
-    spread, gathered = lax.optimization_barrier((spread, gathered))
+    spread = spread.reshape(-1, 2, *packed.shape).astype(jnp.bfloat16)
     core = lax.axis_index("c").astype(jnp.int32)[None]
-    up_own, down_own, pieces = apply(core, gathered, spread.astype(jnp.float32), y_count)
+    up_own, down_own, pieces = apply(core, gathered, spread, units, feat_rows, y_count)
     for groups in crossed_groups(x_count, y_count):
         pieces = lax.all_to_all(
             pieces, ("x", "c", "y"), 0, 0, tiled=True, axis_index_groups=groups

time: 110 us -> 109 us (level)
  starting transfers between devices: 13.7 us -> 8.45 us
  blocking collectives: 79.4 us -> 82.9 us
  Pallas kernels: 8.07 us -> 9.55 us
    all_to_all x1, starting transfers between devices: 10.1 us -> 4.84 us  [on_device(): both = lax.all_to_all(both, 'x', 0, 0, tiled=True)]
    all_gather x1, blocking collectives: 48.5 us -> 51.6 us  [on_device(): spread = lax.all_gather(packed[None], ('z', 'c'), axis=0, tiled=True)]
    pallas_call x2, Pallas kernels: 5.46 us -> 6.97 us  [the longest x1 5.22 us: apply(): pl.pallas_call(functools.partial(apply_kernel, feat_rows), out_shape=(wei...]
  transfers between devices with their start and end apart: 2 -> 2, of which waited for: 1 -> 1; matrix products, arithmetic and copies ran while one was open for 0% -> 3% of each run, Pallas kernels for 2% -> 2%
where the time goes in v5:
time: 109 us; the launch traced here: 108 us
  blocking collectives  82.9 us (76%)
  Pallas kernels  9.55 us (9%)
  starting transfers between devices  8.45 us (8%)
  other arithmetic  4.21 us (4%)
  waiting for transfers between devices  2.24 us (2%)
    all_gather x1, blocking collectives, on_device(): spread = lax.all_gather(packed[None], ('z', 'c'), axis=0, tiled=True)  51.6 us
    all_to_all x2, blocking collectives, on_device(): lax.all_to_all(pieces, ('x', 'c', 'y'), 0, 0, tiled=True, axis_index_grou...  31.3 us
    pallas_call x1, Pallas kernels, apply(): pl.pallas_call(functools.partial(apply_kernel, feat_rows), out_shape=(wei...  5.22 us
    all_to_all x1, starting transfers between devices, on_device(): both = lax.all_to_all(both, 'x', 0, 0, tiled=True)  4.84 us
    all_to_all x1, starting transfers between devices, on_device(): lax.all_to_all(norm_copies(tokens, x_count), 'x', 0, 0, tiled=True)  3.61 us
    convert_element_type x1, other arithmetic, on_device(): spread = spread.reshape(-1, 2, *packed.shape).astype(jnp.bfloat16)  2.69 us
    pallas_call x1, Pallas kernels, norm_copies(): pl.pallas_call(norm_kernel, out_shape=jax.ShapeDtypeStruct((count, *token...  2.58 us
    all_to_all x1, waiting for transfers between devices, on_device(): both = lax.all_to_all(both, 'x', 0, 0, tiled=True)  2.24 us
  transfers between devices with their start and end apart: 2, of which 1 were waited for; matrix products, arithmetic and copies ran while one was open for 3% of the time, Pallas kernels for 2%

profile of v5, /device:TPU:1, one launch (start us, length us, event | category | flops | bytes accessed | tf_op | source)
XLA Modules:
  0.0 108.1 jit_solution(8951239608735148533)
XLA Ops:
  0.6 1.8 %shard_map.68 = bf16[4,8,16,128]{3,2,1,0:T(8,128)(2,1)} custom-call(f32[1,16]{1,0:T(1,128)} %bitcast.49, f32[16,2048]{1,0:T(8,128)} %up_in.1, f32[16,2048]{1,0:T(8,128)} %down_in.1), custom_call_target="tpu_custom_call" | custom-call | flops 65536 | bytes 393216 | tf_op jit(solution)/shard_map/pallas_call | solution.py:60
  2.4 4.8 %all-to-all-start.1 = ((bf16[4,8,16,128]{3,2,1,0:T(8,128)(2,1)}), bf16[4,8,16,128]{3,2,1,0:T(8,128)(2,1)S(1)}, u32[]{:S(2)}, u32[]{:S(2)}) async-start(bf16[4,8,16,128]{3,2,1,0:T(8,128)(2,1)} %shard_map.68), calls=%async_computation.1 | async-start | bytes 262144 | tf_op jit(solution)/shard_map/all_to_all | solution.py:224
  7.2 2.6 %shard_map.67 = bf16[4,128,2048]{2,1,0:T(8,128)(2,1)} custom-call(bf16[128,2048]{1,0:T(8,128)(2,1)} %tokens.1), custom_call_target="tpu_custom_call" | custom-call | flops 2000000000 | bytes 2621440 | tf_op jit(solution)/shard_map/pallas_call | solution.py:88
  9.8 2.2 %all-to-all-done.1 = bf16[4,8,16,128]{3,2,1,0:T(8,128)(2,1)S(1)} async-done(((bf16[4,8,16,128]{3,2,1,0:T(8,128)(2,1)}), bf16[4,8,16,128]{3,2,1,0:T(8,128)(2,1)S(1)}, u32[]{:S(2)}, u32[]{:S(2)}) %all-to-all-start.1) | async-done | bytes 131104 | tf_op jit(solution)/shard_map/all_to_all | solution.py:224
  12.1 3.6 %all-to-all-start = ((bf16[4,128,2048]{2,1,0:T(8,128)(2,1)}), bf16[4,128,2048]{2,1,0:T(8,128)(2,1)S(1)}, u32[]{:S(2)}, u32[]{:S(2)}) async-start(bf16[4,128,2048]{2,1,0:T(8,128)(2,1)} %shard_map.67), calls=%async_computation | async-start | bytes 4194304 | tf_op jit(solution)/shard_map/all_to_all | solution.py:225
  15.9 51.6 %all-gather.1 = f16[32,520,128]{2,1,0:T(8,128)(2,1)S(1)} all-gather(f16[1,520,128]{2,1,0:T(8,128)(2,1)S(1)} %pad_maximum_fusion), channel_id=1, replica_groups=mesh['z'=16,'x'=4,'c'=2,'y'=4] {'z','c'}, dimensions={0}, use_global_device_ids=true | all-gather | bytes 4392960 | tf_op jit(solution)/shard_map/all_gather | solution.py:231
  67.6 2.7 %convert_element_type.21 = bf16[32,520,128]{2,1,0:T(8,128)(2,1)} convert(f16[32,520,128]{2,1,0:T(8,128)(2,1)S(1)} %all-gather.1) | non-fusion elementwise | flops 2129920 | bytes 8519680 | tf_op jit(solution)/shard_map/convert_element_type | solution.py:232
  70.3 0.0 all-to-all-done.tokens
  70.3 5.2 %shard_map.69 = (bf16[2048,256]{1,0:T(8,128)(2,1)}, bf16[2048,256]{1,0:T(8,128)(2,1)}, bf16[16,128,512]{2,1,0:T(8,128)(2,1)S(1)}) custom-call(s32[1]{0:T(128)} %bitcast.core_ref, bf16[4,128,2048]{2,1,0:T(8,128)(2,1)S(1)} %all-to-all-done.tokens, bf16[16,2,520,128]{3,2,1,0:T(8,128)(2,1)} %bitcast.44), custom_call_target="tpu_custom_call" | custom-call | flops 2147483648 | bytes 16777216 | tf_op jit(solution)/shard_map/pallas_call | solution.py:181
  75.5 19.6 %all_to_all.20 = bf16[16,128,512]{2,1,0:T(8,128)(2,1)S(1)} all-to-all(bf16[16,128,512]{2,1,0:T(8,128)(2,1)S(1)} %get-tuple-element.8), channel_id=1, replica_groups={{0,8,16,24},{1,9,17,25},{2,10,18,26},{3,11,19,27},{4,5,6,7},{12,13,14,1..., dimensions={0} | all-to-all | bytes 4194304 | tf_op jit(solution)/shard_map/all_to_all | solution.py:236
  95.1 0.6 reduce_sum.24
  95.7 11.7 %all_to_all.21 = bf16[4,128,512]{2,1,0:T(8,128)(2,1)S(1)} all-to-all(bf16[4,128,512]{2,1,0:T(8,128)(2,1)S(1)} %reduce_sum.24), channel_id=1, replica_groups={{0,1,2,3},{8,9,10,11},{16,17,18,19},{24,25,26,27},{4,12,20,28},{5,13,21..., dimensions={0} | all-to-all | bytes 1048576 | tf_op jit(solution)/shard_map/all_to_all | solution.py:236
  107.4 0.7 reduce_sum.25
  (9 shorter events, 0.2 us)
Async XLA Ops:
  2.4 9.7 %all-to-all-start.1 = ((bf16[4,8,16,128]{3,2,1,0:T(8,128)(2,1)}), bf16[4,8,16,128]{3,2,1,0:T(8,128)(2,1)S(1)}, u32[]{:S(2)}, u32[]{:S(2)}) async-start(bf16[4,8,16,128]{3,2,1,0:T(8,128)(2,1)} %shard_map.68), calls=%async_computation.1 | async-start | bytes 262144 | tf_op jit(solution)/shard_map/all_to_all | solution.py:224
  12.1 58.2 %all-to-all-start = ((bf16[4,128,2048]{2,1,0:T(8,128)(2,1)}), bf16[4,128,2048]{2,1,0:T(8,128)(2,1)S(1)}, u32[]{:S(2)}, u32[]{:S(2)}) async-start(bf16[4,128,2048]{2,1,0:T(8,128)(2,1)} %shard_map.67), calls=%async_computation | async-start | bytes 4194304 | tf_op jit(solution)/shard_map/all_to_all | solution.py:225

commit v6 on v5

--- a/solution.py
+++ b/solution.py
@@ -14,7 +14,7 @@
 ROOM = 2.0**15
 FACTORS = 4
 REACH = 28
-GRANT = 47 << 20
+GRANT = 24 << 20
 
 
 def power_scale(largest):
@@ -100,62 +100,59 @@
 
 
 def apply_kernel(
-    feat_rows, core_ref, tokens, weights, up_out, down_out, pieces, held, up, down, hidden, load_sems, sems
+    feat_rows, core_ref, tokens, weights, up_out, down_out, pieces, up, down, hidden, sems
 ):
     core = core_ref[0]
     x_count, rows, width = tokens.shape
     y_count = pieces.shape[0] // x_count
     part = width // y_count
     units = up_out.shape[1]
-    z_count = held.shape[0]
+    z_count = weights.shape[0]
+    feats = width // z_count
     slab_rows = x_count * feat_rows
     unit_slabs = units // LANES
     slabs = 2 * unit_slabs
     last = 2 * slabs * slab_rows
 
-    def load(z):
-        return pltpu.make_async_copy(weights.at[z], held.at[z], load_sems.at[z])
-
-    for z in range(z_count):
-        load(z).start()
-
-    def unpack(z, carry):
-        load(z).wait()
+    def unpack(z, matrix, target):
         for source in range(2):
-            for matrix, target in enumerate((up, down)):
-                first = last + matrix * FACTORS
-                factors = held[z, source, first : first + FACTORS].astype(jnp.float32)
-                inverse = factors[0:1] * ROOM**-FACTORS
-                for k in range(1, FACTORS):
-                    inverse = inverse * factors[k : k + 1]
-                for half in range(2):
-                    member = core if half == 0 else 1 - core
-                    for j in range(unit_slabs):
-                        slab = matrix * slabs + member * unit_slabs + j
-                        start = pl.multiple_of(slab * slab_rows, slab_rows)
-                        packed = held[z, source, pl.ds(start, slab_rows)].astype(jnp.float32)
-                        values = (packed * inverse).astype(jnp.bfloat16)
-                        column = half * units + j * LANES
-                        for x in range(x_count):
-                            row = ((z * x_count + x) * 2 + source) * feat_rows
-                            target[pl.ds(pl.multiple_of(row, feat_rows), feat_rows), column : column + LANES] = (
-                                values[x * feat_rows : (x + 1) * feat_rows]
-                            )
-        return carry
-
-    lax.fori_loop(0, z_count, unpack, 0)
-    hidden[...] = jnp.zeros_like(hidden)
-    for k in range(y_count):
-        cols = slice(k * part, (k + 1) * part)
-        hidden[...] += jnp.dot(
-            tokens[:, :, cols].reshape(x_count * rows, part),
-            up[cols, :],
-            preferred_element_type=jnp.float32,
-        )
+            first = last + matrix * FACTORS
+            factors = weights[z, source, first : first + FACTORS].astype(jnp.float32)
+            inverse = factors[0:1] * ROOM**-FACTORS
+            for k in range(1, FACTORS):
+                inverse = inverse * factors[k : k + 1]
+            inverse = inverse.astype(jnp.bfloat16)
+            for half in range(2):
+                member = core if half == 0 else 1 - core
+                for j in range(unit_slabs):
+                    slab = matrix * slabs + member * unit_slabs + j
+                    start = pl.multiple_of(slab * slab_rows, slab_rows)
+                    values = weights[z, source, pl.ds(start, slab_rows)] * inverse
+                    column = half * units + j * LANES
+                    for x in range(x_count):
+                        row = ((z * x_count + x) * 2 + source) * feat_rows
+                        target[row : row + feat_rows, column : column + LANES] = values[
+                            x * feat_rows : (x + 1) * feat_rows
+                        ]
+
     copies = [
         pltpu.make_async_copy(source.at[:, :units], target, sems.at[i])
         for i, (source, target) in enumerate(((up, up_out), (down, down_out)))
     ]
+    for first in range(0, z_count, 2):
+        for z in range(first, first + 2):
+            unpack(z, 0, up)
+            unpack(z, 1, down)
+        cols = slice(first * feats, (first + 2) * feats)
+        term = jnp.dot(
+            tokens[:, :, cols].reshape(x_count * rows, 2 * feats),
+            up[cols, :],
+            preferred_element_type=jnp.float32,
+        )
+        if first == 0:
+            hidden[...] = term
+        else:
+            hidden[...] += term
     for copy in copies:
         copy.start()
     act = jnp.square(jnp.maximum(hidden[...], 0.0)).astype(jnp.bfloat16)
@@ -185,14 +182,12 @@
             weight,
             jax.ShapeDtypeStruct((x_count * y_count, rows, width // y_count), jnp.bfloat16),
         ),
-        in_specs=[pl.BlockSpec(memory_space=pltpu.SMEM), vmem, anywhere],
+        in_specs=[pl.BlockSpec(memory_space=pltpu.SMEM), vmem, vmem],
         out_specs=(anywhere, anywhere, vmem),
         scratch_shapes=[
-            pltpu.VMEM(weights.shape, jnp.bfloat16),
             pltpu.VMEM((width, 2 * units), jnp.bfloat16),
             pltpu.VMEM((width, 2 * units), jnp.bfloat16),
             pltpu.VMEM((x_count * rows, 2 * units), jnp.float32),
-            pltpu.SemaphoreType.DMA((weights.shape[0],)),
             pltpu.SemaphoreType.DMA((2,)),
         ],
         cost_estimate=pl.CostEstimate(
@@ -229,6 +224,7 @@
     packed = (block * scale[None, :, None, None]).transpose(1, 2, 0, 3, 4).reshape(-1, LANES)
     packed = jnp.concatenate([packed, factors.reshape(-1, LANES)]).astype(jnp.float16)
     spread = lax.all_gather(packed[None], ("z", "c"), axis=0, tiled=True)
+    spread, gathered = lax.optimization_barrier((spread, gathered))
     spread = spread.reshape(-1, 2, *packed.shape).astype(jnp.bfloat16)
     core = lax.axis_index("c").astype(jnp.int32)[None]
     up_own, down_own, pieces = apply(core, gathered, spread, units, feat_rows, y_count)

time: 109 us -> 109 us (level)
  Pallas kernels: 9.55 us -> 7.76 us
  blocking collectives: 82.9 us -> 84.2 us
    pallas_call x1, Pallas kernels: 5.22 us -> 3.42 us  [apply(): pl.pallas_call(functools.partial(apply_kernel, feat_rows), out_shape=(wei...]
    all_gather x1, blocking collectives: 51.6 us -> 53.1 us  [on_device(): spread = lax.all_gather(packed[None], ('z', 'c'), axis=0, tiled=True)]
  transfers between devices with their start and end apart: 2 -> 2, of which waited for: 1 -> 1; matrix products, arithmetic and copies ran while one was open for 3% -> 0% of each run, Pallas kernels for 2% -> 2%
where the time goes in v6:
time: 109 us; the launch traced here: 108 us
  blocking collectives  84.2 us (77%)
  starting transfers between devices  8.45 us (8%)
  Pallas kernels  7.76 us (7%)
  other arithmetic  4.46 us (4%)
  waiting for transfers between devices  2.24 us (2%)
    all_gather x1, blocking collectives, on_device(): spread = lax.all_gather(packed[None], ('z', 'c'), axis=0, tiled=True)  53.1 us
    all_to_all x2, blocking collectives, on_device(): lax.all_to_all(pieces, ('x', 'c', 'y'), 0, 0, tiled=True, axis_index_grou...  31.1 us
    all_to_all x1, starting transfers between devices, on_device(): both = lax.all_to_all(both, 'x', 0, 0, tiled=True)  4.84 us
    all_to_all x1, starting transfers between devices, on_device(): lax.all_to_all(norm_copies(tokens, x_count), 'x', 0, 0, tiled=True)  3.61 us
    pallas_call x1, Pallas kernels, apply(): pl.pallas_call(functools.partial(apply_kernel, feat_rows), out_shape=(wei...  3.42 us
    convert_element_type x1, other arithmetic, on_device(): spread = spread.reshape(-1, 2, *packed.shape).astype(jnp.bfloat16)  2.94 us
    pallas_call x1, Pallas kernels, norm_copies(): pl.pallas_call(norm_kernel, out_shape=jax.ShapeDtypeStruct((count, *token...  2.58 us
    all_to_all x1, waiting for transfers between devices, on_device(): both = lax.all_to_all(both, 'x', 0, 0, tiled=True)  2.24 us
  transfers between devices with their start and end apart: 2, of which 1 were waited for; matrix products, arithmetic and copies ran while one was open for 0% of the time, Pallas kernels for 2%

profile of v6, /device:TPU:1, one launch (start us, length us, event | category | flops | bytes accessed | tf_op | source)
XLA Modules:
  0.0 107.9 jit_solution(17892683154030198541)
XLA Ops:
  0.6 1.8 %shard_map.67 = bf16[4,8,16,128]{3,2,1,0:T(8,128)(2,1)} custom-call(f32[1,16]{1,0:T(1,128)} %bitcast.49, f32[16,2048]{1,0:T(8,128)} %up_in.1, f32[16,2048]{1,0:T(8,128)} %down_in.1), custom_call_target="tpu_custom_call" | custom-call | flops 65536 | bytes 393216 | tf_op jit(solution)/shard_map/pallas_call | solution.py:60
  2.4 4.8 %all-to-all-start = ((bf16[4,8,16,128]{3,2,1,0:T(8,128)(2,1)}), bf16[4,8,16,128]{3,2,1,0:T(8,128)(2,1)S(1)}, u32[]{:S(2)}, u32[]{:S(2)}) async-start(bf16[4,8,16,128]{3,2,1,0:T(8,128)(2,1)} %shard_map.67), calls=%async_computation | async-start | bytes 262144 | tf_op jit(solution)/shard_map/all_to_all | solution.py:219
  7.2 2.6 %shard_map.68 = bf16[4,128,2048]{2,1,0:T(8,128)(2,1)} custom-call(bf16[128,2048]{1,0:T(8,128)(2,1)} %tokens.1), custom_call_target="tpu_custom_call" | custom-call | flops 2000000000 | bytes 2621440 | tf_op jit(solution)/shard_map/pallas_call | solution.py:88
  9.8 2.2 %all-to-all-done = bf16[4,8,16,128]{3,2,1,0:T(8,128)(2,1)S(1)} async-done(((bf16[4,8,16,128]{3,2,1,0:T(8,128)(2,1)}), bf16[4,8,16,128]{3,2,1,0:T(8,128)(2,1)S(1)}, u32[]{:S(2)}, u32[]{:S(2)}) %all-to-all-start) | async-done | bytes 131104 | tf_op jit(solution)/shard_map/all_to_all | solution.py:219
  12.1 3.6 %all-to-all-start.1 = ((bf16[4,128,2048]{2,1,0:T(8,128)(2,1)}), bf16[4,128,2048]{2,1,0:T(8,128)(2,1)S(1)}, u32[]{:S(2)}, u32[]{:S(2)}) async-start(bf16[4,128,2048]{2,1,0:T(8,128)(2,1)} %shard_map.68), calls=%async_computation.1 | async-start | bytes 4194304 | tf_op jit(solution)/shard_map/all_to_all | solution.py:220
  15.9 53.1 %all-gather.1 = f16[32,520,128]{2,1,0:T(8,128)(2,1)} all-gather(f16[1,520,128]{2,1,0:T(8,128)(2,1)S(1)} %pad_maximum_fusion), channel_id=1, replica_groups=mesh['z'=16,'x'=4,'c'=2,'y'=4] {'z','c'}, dimensions={0}, use_global_device_ids=true | all-gather | bytes 4392960 | tf_op jit(solution)/shard_map/all_gather | solution.py:226
  69.1 0.0 all-to-all-done.1.tokens
  69.1 2.9 %convert_element_type.21 = bf16[32,520,128]{2,1,0:T(8,128)(2,1)S(1)} convert(f16[32,520,128]{2,1,0:T(8,128)(2,1)} %all-gather.1) | non-fusion elementwise | flops 2129920 | bytes 8519680 | tf_op jit(solution)/shard_map/convert_element_type | solution.py:228
  72.0 3.4 %shard_map.69 = (bf16[2048,256]{1,0:T(8,128)(2,1)}, bf16[2048,256]{1,0:T(8,128)(2,1)}, bf16[16,128,512]{2,1,0:T(8,128)(2,1)S(1)}) custom-call(s32[1]{0:T(128)} %bitcast.core_ref, bf16[4,128,2048]{2,1,0:T(8,128)(2,1)S(1)} %all-to-all-done.1.tokens, bf16[16,2,520,128]{3,2,1,0:T(8,128)(2,1)S(1)} %bitcast.43), custom_call_target="tpu_custom_call" | custom-call | flops 2147483648 | bytes 16777216 | tf_op jit(solution)/shard_map/pallas_call | solution.py:178
  75.5 19.6 %all_to_all.20 = bf16[16,128,512]{2,1,0:T(8,128)(2,1)S(1)} all-to-all(bf16[16,128,512]{2,1,0:T(8,128)(2,1)S(1)} %get-tuple-element.12), channel_id=1, replica_groups={{0,8,16,24},{1,9,17,25},{2,10,18,26},{3,11,19,27},{4,5,6,7},{12,13,14,1..., dimensions={0} | all-to-all | bytes 4194304 | tf_op jit(solution)/shard_map/all_to_all | solution.py:232
  95.1 0.6 reduce_sum.24
  95.7 11.4 %all_to_all.21 = bf16[4,128,512]{2,1,0:T(8,128)(2,1)S(1)} all-to-all(bf16[4,128,512]{2,1,0:T(8,128)(2,1)S(1)} %reduce_sum.24), channel_id=1, replica_groups={{0,1,2,3},{8,9,10,11},{16,17,18,19},{24,25,26,27},{4,12,20,28},{5,13,21..., dimensions={0} | all-to-all | bytes 1048576 | tf_op jit(solution)/shard_map/all_to_all | solution.py:232
  107.1 0.7 reduce_sum.25
  (9 shorter events, 0.2 us)
Async XLA Ops:
  2.4 9.7 %all-to-all-start = ((bf16[4,8,16,128]{3,2,1,0:T(8,128)(2,1)}), bf16[4,8,16,128]{3,2,1,0:T(8,128)(2,1)S(1)}, u32[]{:S(2)}, u32[]{:S(2)}) async-start(bf16[4,8,16,128]{3,2,1,0:T(8,128)(2,1)} %shard_map.67), calls=%async_computation | async-start | bytes 262144 | tf_op jit(solution)/shard_map/all_to_all | solution.py:219
  12.1 57.0 %all-to-all-start.1 = ((bf16[4,128,2048]{2,1,0:T(8,128)(2,1)}), bf16[4,128,2048]{2,1,0:T(8,128)(2,1)S(1)}, u32[]{:S(2)}, u32[]{:S(2)}) async-start(bf16[4,128,2048]{2,1,0:T(8,128)(2,1)} %shard_map.68), calls=%async_computation.1 | async-start | bytes 4194304 | tf_op jit(solution)/shard_map/all_to_all | solution.py:220

commit v7 on v6

--- a/solution.py
+++ b/solution.py
@@ -8,6 +8,7 @@
 from jax.experimental.pallas import tpu as pltpu
 from jax.sharding import Mesh
 from jax.sharding import PartitionSpec as P
+
 
 SUB = 8
 LANES = 128
@@ -33,76 +34,71 @@
     return scale, jnp.stack(factors, axis=1)
 
 
-def fold_kernel(gain_in, up_in, down_in, out, gain, up, down, sems):
+def prologue_kernel(x_ref, gain_in, up_in, down_in, tokens_in, *refs):
+    blocks, (copies, gain, up, down, tokens, normed, sems) = refs[:-7], refs[-7:]
+    chips = len(blocks)
     loads = [
         pltpu.make_async_copy(source, target, sems.at[i])
-        for i, (source, target) in enumerate(((gain_in, gain), (up_in, up), (down_in, down)))
+        for i, (source, target) in enumerate(
+            ((tokens_in, tokens), (gain_in, gain), (up_in, up), (down_in, down))
+        )
     ]
     for load in loads:
         load.start()
-    for load in loads:
+    loads[0].wait()
+    widened = tokens[...].astype(jnp.float32)
+    mean = jnp.mean(widened * widened, axis=1, keepdims=True)
+    normed[...] = (widened * lax.rsqrt(mean + 1e-06)).astype(jnp.bfloat16)
+    for load in loads[1:]:
         load.wait()
-    chips, double, rows, _ = out.shape
+    stores = [
+        pltpu.make_async_copy(normed, copies.at[i], sems.at[len(loads) + i]) for i in range(chips)
+    ]
+    for store in stores:
+        store.start()
+    double, rows, _ = blocks[0].shape
     slabs = double // 2
     square = (rows, rows)
     here = lax.broadcasted_iota(jnp.int32, square, 0) == lax.broadcasted_iota(jnp.int32, square, 1)
     spread = jnp.sum(jnp.where(here, jnp.broadcast_to(gain[...], square), 0.0), axis=1, keepdims=True)
-    for x in range(chips):
+    for ahead, block in enumerate(blocks):
+        keeper = lax.rem(x_ref[0] + ahead, chips)
         for slab in range(slabs):
-            first = (x * slabs + slab) * LANES
-            out[x, slab] = (spread * up[:, first : first + LANES]).astype(jnp.bfloat16)
-            out[x, slabs + slab] = down[:, first : first + LANES].astype(jnp.bfloat16)
-
-
-def fold(gain, up, down, chips):
+            at = pl.ds(pl.multiple_of((keeper * slabs + slab) * LANES, LANES), LANES)
+            block[slab] = (spread * up[:, at]).astype(jnp.bfloat16)
+            block[slabs + slab] = down[:, at].astype(jnp.bfloat16)
+    for store in stores:
+        store.wait()
+
+
+def prologue(x, gain, up, down, tokens, chips):
     rows, columns = up.shape
-    slabs = columns // chips // LANES
+    block = jax.ShapeDtypeStruct((2 * columns // chips // LANES, rows, LANES), jnp.bfloat16)
+    anywhere = pl.BlockSpec(memory_space=pl.ANY)
     return pl.pallas_call(
-        fold_kernel,
-        out_shape=jax.ShapeDtypeStruct((chips, 2 * slabs, rows, LANES), jnp.bfloat16),
-        in_specs=[pl.BlockSpec(memory_space=pl.ANY)] * 3,
+        prologue_kernel,
+        out_shape=(block,) * chips
+        + (jax.ShapeDtypeStruct((chips, *tokens.shape), jnp.bfloat16),),
+        in_specs=[pl.BlockSpec(memory_space=pltpu.SMEM)] + [anywhere] * 4,
+        out_specs=(pl.BlockSpec(memory_space=pltpu.VMEM),) * chips + (anywhere,),
         scratch_shapes=[
             pltpu.VMEM(gain.shape, jnp.float32),
             pltpu.VMEM(up.shape, jnp.float32),
             pltpu.VMEM(up.shape, jnp.float32),
-            pltpu.SemaphoreType.DMA((3,)),
+            pltpu.VMEM(tokens.shape, jnp.bfloat16),
+            pltpu.VMEM(tokens.shape, jnp.bfloat16),
+            pltpu.SemaphoreType.DMA((4 + chips,)),
         ],
         cost_estimate=pl.CostEstimate(
-            flops=2 * up.size, bytes_accessed=12 * up.size, transcendentals=0
+            flops=10 * tokens.size, bytes_accessed=10 * tokens.size, transcendentals=tokens.shape[0]
         ),
-    )(gain, up, down)
-
-
-def norm_kernel(tokens, out, normed, sems):
-    widened = tokens[...].astype(jnp.float32)
-    mean = jnp.mean(widened * widened, axis=1, keepdims=True)
-    normed[...] = (widened * lax.rsqrt(mean + 1e-06)).astype(jnp.bfloat16)
-    copies = [pltpu.make_async_copy(normed, out.at[x], sems.at[x]) for x in range(out.shape[0])]
-    for copy in copies:
-        copy.start()
-    for copy in copies:
-        copy.wait()
-
-
-def norm_copies(tokens, count):
-    return pl.pallas_call(
-        norm_kernel,
-        out_shape=jax.ShapeDtypeStruct((count, *tokens.shape), jnp.bfloat16),
-        out_specs=pl.BlockSpec(memory_space=pltpu.HBM),
-        scratch_shapes=[
-            pltpu.VMEM(tokens.shape, jnp.bfloat16),
-            pltpu.SemaphoreType.DMA((count,)),
-        ],
-        cost_estimate=pl.CostEstimate(
-            flops=2_000_000_000, bytes_accessed=10 * tokens.size, transcendentals=tokens.shape[0]
-        ),
-    )(tokens)
+    )(x, gain, up, down, tokens)
 
 
 def apply_kernel(
-    feat_rows, core_ref, tokens, weights, up_out, down_out, pieces, up, down, hidden, sems
+    feat_rows, place_ref, tokens, weights, up_out, down_out, pieces, up, down, hidden, sems
 ):
-    core = core_ref[0]
+    core, chip = place_ref[0], place_ref[1]
     x_count, rows, width = tokens.shape
     y_count = pieces.shape[0] // x_count
     part = width // y_count
@@ -129,11 +125,12 @@
                     start = pl.multiple_of(slab * slab_rows, slab_rows)
                     values = weights[z, source, pl.ds(start, slab_rows)] * inverse
                     column = half * units + j * LANES
-                    for x in range(x_count):
-                        row = ((z * x_count + x) * 2 + source) * feat_rows
-                        target[row : row + feat_rows, column : column + LANES] = values[
-                            x * feat_rows : (x + 1) * feat_rows
-                        ]
+                    for behind in range(x_count):
+                        sender = lax.rem(chip + x_count - behind, x_count)
+                        row = ((z * x_count + sender) * 2 + source) * feat_rows
+                        target[
+                            pl.ds(pl.multiple_of(row, feat_rows), feat_rows), column : column + LANES
+                        ] = values[behind * feat_rows : (behind + 1) * feat_rows]
 
     copies = [
         pltpu.make_async_copy(source.at[:, :units], target, sems.at[i])
@@ -170,7 +167,7 @@
         copy.wait()
 
 
-def apply(core, tokens, weights, units, feat_rows, y_count):
+def apply(place, tokens, weights, units, feat_rows, y_count):
     x_count, rows, width = tokens.shape
     weight = jax.ShapeDtypeStruct((width, units), jnp.bfloat16)
     vmem = pl.BlockSpec(memory_space=pltpu.VMEM)
@@ -194,7 +191,7 @@
             flops=8 * x_count * rows * width * units, bytes_accessed=16 << 20, transcendentals=0
         ),
         compiler_params=pltpu.CompilerParams(vmem_limit_bytes=GRANT),
-    )(core, tokens, weights)
+    )(place, tokens, weights)
 
 
 def crossed_groups(x_count, y_count):
@@ -215,19 +212,23 @@
     units = up_master.shape[1] // SUB
     x_count = lax.axis_size("x")
     y_count = lax.axis_size("y")
-    both = fold(gain[None], up_master, down_master, x_count)
-    both = lax.all_to_all(both, "x", 0, 0, tiled=True)
-    gathered = lax.all_to_all(norm_copies(tokens, x_count), "x", 0, 0, tiled=True)
-
-    block = both.astype(jnp.float32).reshape(x_count, 2, -1, feat_rows, LANES)
+    chip = lax.axis_index("x").astype(jnp.int32)
+    *blocks, copies = prologue(chip[None], gain[None], up_master, down_master, tokens, x_count)
+    for ahead in range(1, x_count):
+        blocks[ahead] = lax.ppermute(
+            blocks[ahead], "x", [(i, (i + ahead) % x_count) for i in range(x_count)]
+        )
+    gathered = lax.all_to_all(copies, "x", 0, 0, tiled=True)
+
+    block = jnp.stack(blocks).astype(jnp.float32).reshape(x_count, 2, -1, feat_rows, LANES)
     scale, factors = power_scale(jnp.max(jnp.abs(block), axis=(0, 2, 3)))
     packed = (block * scale[None, :, None, None]).transpose(1, 2, 0, 3, 4).reshape(-1, LANES)
     packed = jnp.concatenate([packed, factors.reshape(-1, LANES)]).astype(jnp.float16)
     spread = lax.all_gather(packed[None], ("z", "c"), axis=0, tiled=True)
     spread, gathered = lax.optimization_barrier((spread, gathered))
     spread = spread.reshape(-1, 2, *packed.shape).astype(jnp.bfloat16)
-    core = lax.axis_index("c").astype(jnp.int32)[None]
-    up_own, down_own, pieces = apply(core, gathered, spread, units, feat_rows, y_count)
+    place = jnp.stack([lax.axis_index("c").astype(jnp.int32), chip])
+    up_own, down_own, pieces = apply(place, gathered, spread, units, feat_rows, y_count)
     for groups in crossed_groups(x_count, y_count):
         pieces = lax.all_to_all(
             pieces, ("x", "c", "y"), 0, 0, tiled=True, axis_index_groups=groups

time: 109 us -> 127 us (1.17)
  waiting for transfers between devices: 2.24 us -> 11.4 us
  starting transfers between devices: 8.45 us -> 15.7 us
  blocking collectives: 84.2 us -> 86.7 us
    ppermute x0 -> x3, waiting for transfers between devices: none -> 11.4 us  [on_device(): lax.ppermute(blocks[ahead], 'x', [(i, (i + ahead) % x_count) for i in ran...]
    ppermute x0 -> x3, starting transfers between devices: none -> 10.8 us  [on_device(): lax.ppermute(blocks[ahead], 'x', [(i, (i + ahead) % x_count) for i in ran...]
    all_gather x1, blocking collectives: 53.1 us -> 57.8 us  [on_device(): spread = lax.all_gather(packed[None], ('z', 'c'), axis=0, tiled=True)]
    all_to_all x2 -> x1, starting transfers between devices: 8.45 us -> 4.97 us  [on_device(): gathered = lax.all_to_all(copies, 'x', 0, 0, tiled=True)]
    all_to_all x2 -> x1, waiting for transfers between devices: 2.24 us -> 0.01 us  [on_device(): gathered = lax.all_to_all(copies, 'x', 0, 0, tiled=True)]
    all_to_all x2, blocking collectives: 31.1 us -> 29 us  [on_device(): lax.all_to_all(pieces, ('x', 'c', 'y'), 0, 0, tiled=True, axis_index_grou...]
    pallas_call x2 -> x1, Pallas kernels: 4.33 us -> 3.3 us  [prologue(): pl.pallas_call(prologue_kernel, out_shape=(block,) * chips + (jax.ShapeDt...]
  transfers between devices with their start and end apart: 2 -> 4, of which waited for: 1 -> 2; matrix products, arithmetic and copies ran while one was open for 0% -> 0% of each run, Pallas kernels for 2% -> 0%
where the time goes in v7:
time: 127 us
  blocking collectives  86.7 us (68%)
  starting transfers between devices  15.7 us (12%)
  waiting for transfers between devices  11.4 us (9%)
  Pallas kernels  7.55 us (6%)
  other arithmetic  4.55 us (4%)
    all_gather x1, blocking collectives, on_device(): spread = lax.all_gather(packed[None], ('z', 'c'), axis=0, tiled=True)  57.8 us
    all_to_all x2, blocking collectives, on_device(): lax.all_to_all(pieces, ('x', 'c', 'y'), 0, 0, tiled=True, axis_index_grou...  29 us
    ppermute x3, waiting for transfers between devices, on_device(): lax.ppermute(blocks[ahead], 'x', [(i, (i + ahead) % x_count) for i in ran...  11.4 us
    ppermute x3, starting transfers between devices, on_device(): lax.ppermute(blocks[ahead], 'x', [(i, (i + ahead) % x_count) for i in ran...  10.8 us
    all_to_all x1, starting transfers between devices, on_device(): gathered = lax.all_to_all(copies, 'x', 0, 0, tiled=True)  4.97 us
    pallas_call x1, Pallas kernels, apply(): pl.pallas_call(functools.partial(apply_kernel, feat_rows), out_shape=(wei...  4.25 us
    pallas_call x1, Pallas kernels, prologue(): pl.pallas_call(prologue_kernel, out_shape=(block,) * chips + (jax.ShapeDt...  3.3 us
    convert_element_type x1, other arithmetic, on_device(): spread = spread.reshape(-1, 2, *packed.shape).astype(jnp.bfloat16)  2.94 us
  transfers between devices with their start and end apart: 4, of which 2 were waited for; matrix products, arithmetic and copies ran while one was open for 0% of the time, Pallas kernels for 0%

profile of v7, /device:TPU:1, one launch (start us, length us, event | category | flops | bytes accessed | tf_op | source)
XLA Modules:
  0.0 126.8 jit_solution(15182775326017180412)
XLA Ops:
  0.6 3.3 %shard_map.67 = (bf16[8,16,128]{2,1,0:T(8,128)(2,1)}, bf16[8,16,128]{2,1,0:T(8,128)(2,1)}, bf16[8,16,128]{2,1,0:T(8,128)(2,1)}, bf16[8,16,128]{2,1,0:T(8,128)(2,1)}, bf16[4,128,2048]{2,1,0:T(8,128)(2,1)}) custom-call(s32[1]{0:T(128)} %bitcast.1.x_ref, f32[1,16]{1,0:T(1,128)} %bitcast.30, f32[16,2048]{1,0:T(8,128)} %up_in.1, f32[16,2048]{1,0:T(8,128)} %down_in.1, ...), custom_call_target="tpu_custom_call" | custom-call | flops 2621440 | bytes 2621440 | tf_op jit(solution)/shard_map/pallas_call | solution.py:78
  3.9 0.0 copy-start.3
  4.0 0.0 copy-start.2
  4.0 0.0 copy-start.1
  4.0 0.0 copy-start
  4.0 5.0 %all-to-all-start = ((bf16[4,128,2048]{2,1,0:T(8,128)(2,1)}), bf16[4,128,2048]{2,1,0:T(8,128)(2,1)S(1)}, u32[]{:S(2)}, u32[]{:S(2)}) async-start(bf16[4,128,2048]{2,1,0:T(8,128)(2,1)} %get-tuple-element.17), calls=%async_computation | async-start | bytes 4194304 | tf_op jit(solution)/shard_map/all_to_all | solution.py:221
  9.0 0.0 copy-done.3
  9.0 3.4 %collective-permute-start = (bf16[8,16,128]{2,1,0:T(8,128)(2,1)S(1)}, bf16[8,16,128]{2,1,0:T(8,128)(2,1)S(1)}, u32[]{:S(2)}, u32[]{:S(2)}) collective-permute-start(bf16[8,16,128]{2,1,0:T(8,128)(2,1)S(1)} %copy-done.3), channel_id=1, source_target_pairs={{0,8},{8,16},{16,24},{24,0},{1,9},{9,17},{17,25},{25,1},{2,10},{10... | collective-permute-start | bytes 98312 | tf_op jit(solution)/shard_map/ppermute | solution.py:218
  12.3 0.0 copy-done.2
  12.3 4.3 %collective-permute-start.1 = (bf16[8,16,128]{2,1,0:T(8,128)(2,1)S(1)}, bf16[8,16,128]{2,1,0:T(8,128)(2,1)S(1)}, u32[]{:S(2)}, u32[]{:S(2)}) collective-permute-start(bf16[8,16,128]{2,1,0:T(8,128)(2,1)S(1)} %copy-done.2), channel_id=1, source_target_pairs={{0,16},{8,24},{16,0},{24,8},{1,17},{9,25},{17,1},{25,9},{2,18},{10... | collective-permute-start | bytes 98312 | tf_op jit(solution)/shard_map/ppermute | solution.py:218
  16.7 3.1 %collective-permute-start.2 = (bf16[8,16,128]{2,1,0:T(8,128)(2,1)S(1)}, bf16[8,16,128]{2,1,0:T(8,128)(2,1)S(1)}, u32[]{:S(2)}, u32[]{:S(2)}) collective-permute-start(bf16[8,16,128]{2,1,0:T(8,128)(2,1)S(1)} %copy-done.1), channel_id=1, source_target_pairs={{0,24},{8,0},{16,8},{24,16},{1,25},{9,1},{17,9},{25,17},{2,26},{10... | collective-permute-start | bytes 98312 | tf_op jit(solution)/shard_map/ppermute | solution.py:218
  19.8 0.1 pad_add_fusion.place_ref
  19.8 7.2 %collective-permute-done = bf16[8,16,128]{2,1,0:T(8,128)(2,1)S(1)} collective-permute-done((bf16[8,16,128]{2,1,0:T(8,128)(2,1)S(1)}, bf16[8,16,128]{2,1,0:T(8,128)(2,1)S(1)}, u32[]{:S(2)}, u32[]{:S(2)}) %collective-permute-start) | collective-permute-done | bytes 32800 | tf_op jit(solution)/shard_map/ppermute | solution.py:218
  27.1 4.1 %collective-permute-done.1 = bf16[8,16,128]{2,1,0:T(8,128)(2,1)S(1)} collective-permute-done((bf16[8,16,128]{2,1,0:T(8,128)(2,1)S(1)}, bf16[8,16,128]{2,1,0:T(8,128)(2,1)S(1)}, u32[]{:S(2)}, u32[]{:S(2)}) %collective-permute-start.1) | collective-permute-done | bytes 32800 | tf_op jit(solution)/shard_map/ppermute | solution.py:218
  31.2 0.0 collective-permute-done.2
  31.3 0.1 fusion.2
  31.5 57.8 %all-gather.1 = f16[32,520,128]{2,1,0:T(8,128)(2,1)} all-gather(f16[1,520,128]{2,1,0:T(8,128)(2,1)S(1)} %pad_maximum_fusion), channel_id=1, replica_groups=mesh['z'=16,'x'=4,'c'=2,'y'=4] {'z','c'}, dimensions={0}, use_global_device_ids=true | all-gather | bytes 4392960 | tf_op jit(solution)/shard_map/all_gather | solution.py:227
  89.2 0.0 all-to-all-done.tokens
  89.2 2.9 %convert_element_type.22 = bf16[32,520,128]{2,1,0:T(8,128)(2,1)S(1)} convert(f16[32,520,128]{2,1,0:T(8,128)(2,1)} %all-gather.1) | non-fusion elementwise | flops 2129920 | bytes 8519680 | tf_op jit(solution)/shard_map/convert_element_type | solution.py:229
  92.2 4.2 %shard_map.68 = (bf16[2048,256]{1,0:T(8,128)(2,1)}, bf16[2048,256]{1,0:T(8,128)(2,1)}, bf16[16,128,512]{2,1,0:T(8,128)(2,1)S(1)}) custom-call(s32[2]{0:T(128)S(1)} %pad_add_fusion.place_ref, bf16[4,128,2048]{2,1,0:T(8,128)(2,1)S(1)} %all-to-all-done.tokens, bf16[16,2,520,128]{3,2,1,0:T(8,128)(2,1)S(1)} %bitcast.16), custom_call_target="tpu_custom_call" | custom-call | flops 2147483648 | bytes 16777216 | tf_op jit(solution)/shard_map/pallas_call | solution.py:175
  96.4 19.3 %all_to_all.15 = bf16[16,128,512]{2,1,0:T(8,128)(2,1)S(1)} all-to-all(bf16[16,128,512]{2,1,0:T(8,128)(2,1)S(1)} %get-tuple-element.22), channel_id=1, replica_groups={{0,8,16,24},{1,9,17,25},{2,10,18,26},{3,11,19,27},{4,5,6,7},{12,13,14,1..., dimensions={0} | all-to-all | bytes 4194304 | tf_op jit(solution)/shard_map/all_to_all | solution.py:233
  115.8 0.6 reduce_sum.24
  116.4 9.6 %all_to_all.16 = bf16[4,128,512]{2,1,0:T(8,128)(2,1)S(1)} all-to-all(bf16[4,128,512]{2,1,0:T(8,128)(2,1)S(1)} %reduce_sum.24), channel_id=1, replica_groups={{0,1,2,3},{8,9,10,11},{16,17,18,19},{24,25,26,27},{4,12,20,28},{5,13,21..., dimensions={0} | all-to-all | bytes 1048576 | tf_op jit(solution)/shard_map/all_to_all | solution.py:233
  126.0 0.7 reduce_sum.25
  (9 shorter events, 0.2 us)
Async XLA Ops:
  3.9 5.0 %copy-start.3 = (bf16[8,16,128]{2,1,0:T(8,128)(2,1)S(1)}, bf16[8,16,128]{2,1,0:T(8,128)(2,1)}, u32[]{:S(2)}) copy-start(bf16[8,16,128]{2,1,0:T(8,128)(2,1)} %get-tuple-element.14) | copy-start | bytes 98308
  4.0 8.4 %copy-start.2 = (bf16[8,16,128]{2,1,0:T(8,128)(2,1)S(1)}, bf16[8,16,128]{2,1,0:T(8,128)(2,1)}, u32[]{:S(2)}) copy-start(bf16[8,16,128]{2,1,0:T(8,128)(2,1)} %get-tuple-element.15) | copy-start | bytes 98308
  4.0 12.7 %copy-start.1 = (bf16[8,16,128]{2,1,0:T(8,128)(2,1)S(1)}, bf16[8,16,128]{2,1,0:T(8,128)(2,1)}, u32[]{:S(2)}) copy-start(bf16[8,16,128]{2,1,0:T(8,128)(2,1)} %get-tuple-element.16) | copy-start | bytes 98308
  4.0 27.2 %copy-start = (bf16[8,16,128]{2,1,0:T(8,128)(2,1)S(1)}, bf16[8,16,128]{2,1,0:T(8,128)(2,1)}, u32[]{:S(2)}) copy-start(bf16[8,16,128]{2,1,0:T(8,128)(2,1)} %get-tuple-element.13) | copy-start | bytes 98308
  4.0 85.2 %all-to-all-start = ((bf16[4,128,2048]{2,1,0:T(8,128)(2,1)}), bf16[4,128,2048]{2,1,0:T(8,128)(2,1)S(1)}, u32[]{:S(2)}, u32[]{:S(2)}) async-start(bf16[4,128,2048]{2,1,0:T(8,128)(2,1)} %get-tuple-element.17), calls=%async_computation | async-start | bytes 4194304 | tf_op jit(solution)/shard_map/all_to_all | solution.py:221
  9.0 18.1 %collective-permute-start = (bf16[8,16,128]{2,1,0:T(8,128)(2,1)S(1)}, bf16[8,16,128]{2,1,0:T(8,128)(2,1)S(1)}, u32[]{:S(2)}, u32[]{:S(2)}) collective-permute-start(bf16[8,16,128]{2,1,0:T(8,128)(2,1)S(1)} %copy-done.3), channel_id=1, source_target_pairs={{0,8},{8,16},{16,24},{24,0},{1,9},{9,17},{17,25},{25,1},{2,10},{10... | collective-permute-start | bytes 98312 | tf_op jit(solution)/shard_map/ppermute | solution.py:218
  12.3 18.9 %collective-permute-start.1 = (bf16[8,16,128]{2,1,0:T(8,128)(2,1)S(1)}, bf16[8,16,128]{2,1,0:T(8,128)(2,1)S(1)}, u32[]{:S(2)}, u32[]{:S(2)}) collective-permute-start(bf16[8,16,128]{2,1,0:T(8,128)(2,1)S(1)} %copy-done.2), channel_id=1, source_target_pairs={{0,16},{8,24},{16,0},{24,8},{1,17},{9,25},{17,1},{25,9},{2,18},{10... | collective-permute-start | bytes 98312 | tf_op jit(solution)/shard_map/ppermute | solution.py:218
  16.7 14.5 %collective-permute-start.2 = (bf16[8,16,128]{2,1,0:T(8,128)(2,1)S(1)}, bf16[8,16,128]{2,1,0:T(8,128)(2,1)S(1)}, u32[]{:S(2)}, u32[]{:S(2)}) collective-permute-start(bf16[8,16,128]{2,1,0:T(8,128)(2,1)S(1)} %copy-done.1), channel_id=1, source_target_pairs={{0,24},{8,0},{16,8},{24,16},{1,25},{9,1},{17,9},{25,17},{2,26},{10... | collective-permute-start | bytes 98312 | tf_op jit(solution)/shard_map/ppermute | solution.py:218

commit v8 on v6

--- a/solution.py
+++ b/solution.py
@@ -8,6 +8,7 @@
 from jax.experimental.pallas import tpu as pltpu
 from jax.sharding import Mesh
 from jax.sharding import PartitionSpec as P
+
 
 SUB = 8
 LANES = 128
@@ -73,37 +74,18 @@
     )(gain, up, down)
 
 
-def norm_kernel(tokens, out, normed, sems):
-    widened = tokens[...].astype(jnp.float32)
-    mean = jnp.mean(widened * widened, axis=1, keepdims=True)
-    normed[...] = (widened * lax.rsqrt(mean + 1e-06)).astype(jnp.bfloat16)
-    copies = [pltpu.make_async_copy(normed, out.at[x], sems.at[x]) for x in range(out.shape[0])]
-    for copy in copies:
-        copy.start()
-    for copy in copies:
-        copy.wait()
-
-
-def norm_copies(tokens, count):
-    return pl.pallas_call(
-        norm_kernel,
-        out_shape=jax.ShapeDtypeStruct((count, *tokens.shape), jnp.bfloat16),
-        out_specs=pl.BlockSpec(memory_space=pltpu.HBM),
-        scratch_shapes=[
-            pltpu.VMEM(tokens.shape, jnp.bfloat16),
-            pltpu.SemaphoreType.DMA((count,)),
-        ],
-        cost_estimate=pl.CostEstimate(
-            flops=2_000_000_000, bytes_accessed=10 * tokens.size, transcendentals=tokens.shape[0]
-        ),
-    )(tokens)
+def norm_factor(tokens):
+    widened = tokens.astype(jnp.float32)
+    return lax.rsqrt(jnp.mean(widened * widened, axis=1, keepdims=True) + 1e-06)
 
 
 def apply_kernel(
-    feat_rows, core_ref, tokens, weights, up_out, down_out, pieces, up, down, hidden, sems
+    feat_rows, place_ref, *refs
 ):
-    core = core_ref[0]
-    x_count, rows, width = tokens.shape
+    *tokens, weights, up_out, down_out, pieces, up, down, hidden, sems = refs
+    core, chip = place_ref[0], place_ref[1]
+    x_count = len(tokens)
+    rows, width = tokens[0].shape
     y_count = pieces.shape[0] // x_count
     part = width // y_count
     units = up_out.shape[1]
@@ -145,7 +127,7 @@
             unpack(z, 1, down)
         cols = slice(first * feats, (first + 2) * feats)
         term = jnp.dot(
-            tokens[:, :, cols].reshape(x_count * rows, 2 * feats),
+            jnp.concatenate([block[:, cols] for block in tokens]),
             up[cols, :],
             preferred_element_type=jnp.float32,
         )
@@ -155,7 +137,8 @@
             hidden[...] += term
     for copy in copies:
         copy.start()
-    act = jnp.square(jnp.maximum(hidden[...], 0.0)).astype(jnp.bfloat16)
+    factor = jnp.concatenate([norm_factor(block[...]) for block in tokens])
+    act = jnp.square(jnp.maximum(hidden[...] * factor, 0.0)).astype(jnp.bfloat16)
     for y in range(y_count):
         out = lax.dot_general(
             act,
@@ -163,15 +146,17 @@
             (((1,), (1,)), ((), ())),
             preferred_element_type=jnp.float32,
         ).astype(jnp.bfloat16)
-        for x in range(x_count):
+        for ahead in range(x_count):
+            x = lax.rem(chip + ahead, x_count)
             place = jnp.where(core == 0, x * y_count + y, y * x_count + x)
-            pieces[place] = out[x * rows : (x + 1) * rows]
+            pieces[place] = out[ahead * rows : (ahead + 1) * rows]
     for copy in copies:
         copy.wait()
 
 
-def apply(core, tokens, weights, units, feat_rows, y_count):
-    x_count, rows, width = tokens.shape
+def apply(place, tokens, weights, units, feat_rows, y_count):
+    x_count = len(tokens)
+    rows, width = tokens[0].shape
     weight = jax.ShapeDtypeStruct((width, units), jnp.bfloat16)
     vmem = pl.BlockSpec(memory_space=pltpu.VMEM)
     anywhere = pl.BlockSpec(memory_space=pl.ANY)
@@ -182,7 +167,7 @@
             weight,
             jax.ShapeDtypeStruct((x_count * y_count, rows, width // y_count), jnp.bfloat16),
         ),
-        in_specs=[pl.BlockSpec(memory_space=pltpu.SMEM), vmem, vmem],
+        in_specs=[pl.BlockSpec(memory_space=pltpu.SMEM)] + [vmem] * (x_count + 1),
         out_specs=(anywhere, anywhere, vmem),
         scratch_shapes=[
             pltpu.VMEM((width, 2 * units), jnp.bfloat16),
@@ -194,7 +179,7 @@
             flops=8 * x_count * rows * width * units, bytes_accessed=16 << 20, transcendentals=0
         ),
         compiler_params=pltpu.CompilerParams(vmem_limit_bytes=GRANT),
-    )(core, tokens, weights)
+    )(place, *tokens, weights)
 
 
 def crossed_groups(x_count, y_count):
@@ -216,18 +201,19 @@
     x_count = lax.axis_size("x")
     y_count = lax.axis_size("y")
     both = fold(gain[None], up_master, down_master, x_count)
+    held = [tokens]
     both = lax.all_to_all(both, "x", 0, 0, tiled=True)
-    gathered = lax.all_to_all(norm_copies(tokens, x_count), "x", 0, 0, tiled=True)
+    for ahead in range(1, x_count):
+        held.append(lax.ppermute(tokens, "x", [((i + ahead) % x_count, i) for i in range(x_count)]))
 
     block = both.astype(jnp.float32).reshape(x_count, 2, -1, feat_rows, LANES)
     scale, factors = power_scale(jnp.max(jnp.abs(block), axis=(0, 2, 3)))
     packed = (block * scale[None, :, None, None]).transpose(1, 2, 0, 3, 4).reshape(-1, LANES)
     packed = jnp.concatenate([packed, factors.reshape(-1, LANES)]).astype(jnp.float16)
     spread = lax.all_gather(packed[None], ("z", "c"), axis=0, tiled=True)
-    spread, gathered = lax.optimization_barrier((spread, gathered))
     spread = spread.reshape(-1, 2, *packed.shape).astype(jnp.bfloat16)
-    core = lax.axis_index("c").astype(jnp.int32)[None]
-    up_own, down_own, pieces = apply(core, gathered, spread, units, feat_rows, y_count)
+    place = jnp.stack([lax.axis_index(axis).astype(jnp.int32) for axis in ("c", "x")])
+    up_own, down_own, pieces = apply(place, held, spread, units, feat_rows, y_count)
     for groups in crossed_groups(x_count, y_count):
         pieces = lax.all_to_all(
             pieces, ("x", "c", "y"), 0, 0, tiled=True, axis_index_groups=groups

time: 109 us -> 123 us (1.13)
  waiting for transfers between devices: 2.24 us -> 19.6 us
  starting transfers between devices: 8.45 us -> 13.5 us
  blocking collectives: 84.2 us -> 79.9 us
  other arithmetic: 4.46 us -> 2.33 us
  Pallas kernels: 7.76 us -> 6.17 us
    all_to_all x1, waiting for transfers between devices: 2.24 us -> 19.6 us  [on_device(): both = lax.all_to_all(both, 'x', 0, 0, tiled=True)]
    ppermute x0 -> x3, starting transfers between devices: none -> 10.2 us  [on_device(): lax.ppermute(tokens, 'x', [((i + ahead) % x_count, i) for i in range(x_co...]
    all_to_all x1 -> x0, starting transfers between devices: 3.61 us -> none  [on_device(): lax.all_to_all(norm_copies(tokens, x_count), 'x', 0, 0, tiled=True)]
    pallas_call x1 -> x0, Pallas kernels: 2.58 us -> none  [norm_copies(): pl.pallas_call(norm_kernel, out_shape=jax.ShapeDtypeStruct((count, *token...]
    all_gather x1, blocking collectives: 53.1 us -> 50.9 us  [on_device(): spread = lax.all_gather(packed[None], ('z', 'c'), axis=0, tiled=True)]
    convert_element_type x1, other arithmetic: 2.94 us -> 0.73 us  [on_device(): spread = spread.reshape(-1, 2, *packed.shape).astype(jnp.bfloat16)]
    all_to_all x2, blocking collectives: 31.1 us -> 29 us  [on_device(): lax.all_to_all(pieces, ('x', 'c', 'y'), 0, 0, tiled=True, axis_index_grou...]
    all_to_all x1, starting transfers between devices: 4.84 us -> 3.35 us  [on_device(): both = lax.all_to_all(both, 'x', 0, 0, tiled=True)]
  transfers between devices with their start and end apart: 2 -> 4, of which waited for: 1 -> 1; matrix products, arithmetic and copies ran while one was open for 0% -> 1% of each run, Pallas kernels for 2% -> 1%
where the time goes in v8:
time: 123 us
  blocking collectives  79.9 us (65%)
  waiting for transfers between devices  19.6 us (16%)
  starting transfers between devices  13.5 us (11%)
  Pallas kernels  6.17 us (5%)
  other arithmetic  2.33 us (2%)
    all_gather x1, blocking collectives, on_device(): spread = lax.all_gather(packed[None], ('z', 'c'), axis=0, tiled=True)  50.9 us
    all_to_all x2, blocking collectives, on_device(): lax.all_to_all(pieces, ('x', 'c', 'y'), 0, 0, tiled=True, axis_index_grou...  29 us
    all_to_all x1, waiting for transfers between devices, on_device(): both = lax.all_to_all(both, 'x', 0, 0, tiled=True)  19.6 us
    ppermute x3, starting transfers between devices, on_device(): lax.ppermute(tokens, 'x', [((i + ahead) % x_count, i) for i in range(x_co...  10.2 us
    pallas_call x1, Pallas kernels, apply(): pl.pallas_call(functools.partial(apply_kernel, feat_rows), out_shape=(wei...  4.42 us
    all_to_all x1, starting transfers between devices, on_device(): both = lax.all_to_all(both, 'x', 0, 0, tiled=True)  3.35 us
  transfers between devices with their start and end apart: 4, of which 1 were waited for; matrix products, arithmetic and copies ran while one was open for 1% of the time, Pallas kernels for 1%

profile of v8, /device:TPU:1, one launch (start us, length us, event | category | flops | bytes accessed | tf_op | source)
XLA Modules:
  0.0 122.6 jit_solution(5247527716745649165)
XLA Ops:
  0.6 5.2 %collective-permute-start = (bf16[128,2048]{1,0:T(8,128)(2,1)}, bf16[128,2048]{1,0:T(8,128)(2,1)S(1)}, u32[]{:S(2)}, u32[]{:S(2)}) collective-permute-start(bf16[128,2048]{1,0:T(8,128)(2,1)} %refs_0_.1), channel_id=1, source_target_pairs={{8,0},{16,8},{24,16},{0,24},{9,1},{17,9},{25,17},{1,25},{10,2},{18... | collective-permute-start | bytes 1572872 | tf_op jit(solution)/shard_map/ppermute | solution.py:207
  5.8 2.4 %collective-permute-start.1 = (bf16[128,2048]{1,0:T(8,128)(2,1)}, bf16[128,2048]{1,0:T(8,128)(2,1)S(1)}, u32[]{:S(2)}, u32[]{:S(2)}) collective-permute-start(bf16[128,2048]{1,0:T(8,128)(2,1)} %refs_0_.1), channel_id=1, source_target_pairs={{16,0},{24,8},{0,16},{8,24},{17,1},{25,9},{1,17},{9,25},{18,2},{26... | collective-permute-start | bytes 1572872 | tf_op jit(solution)/shard_map/ppermute | solution.py:207
  8.3 2.5 %collective-permute-start.2 = (bf16[128,2048]{1,0:T(8,128)(2,1)}, bf16[128,2048]{1,0:T(8,128)(2,1)S(1)}, u32[]{:S(2)}, u32[]{:S(2)}) collective-permute-start(bf16[128,2048]{1,0:T(8,128)(2,1)} %refs_0_.1), channel_id=1, source_target_pairs={{24,0},{0,8},{8,16},{16,24},{25,1},{1,9},{9,17},{17,25},{26,2},{2,... | collective-permute-start | bytes 1572872 | tf_op jit(solution)/shard_map/ppermute | solution.py:207
  10.8 1.8 %shard_map.67 = bf16[4,8,16,128]{3,2,1,0:T(8,128)(2,1)} custom-call(f32[1,16]{1,0:T(1,128)} %bitcast.50, f32[16,2048]{1,0:T(8,128)} %up_in.1, f32[16,2048]{1,0:T(8,128)} %down_in.1), custom_call_target="tpu_custom_call" | custom-call | flops 65536 | bytes 393216 | tf_op jit(solution)/shard_map/pallas_call | solution.py:61
  12.6 3.4 %all-to-all-start = ((bf16[4,8,16,128]{3,2,1,0:T(8,128)(2,1)}), bf16[4,8,16,128]{3,2,1,0:T(8,128)(2,1)S(1)}, u32[]{:S(2)}, u32[]{:S(2)}) async-start(bf16[4,8,16,128]{3,2,1,0:T(8,128)(2,1)} %shard_map.67), calls=%async_computation | async-start | bytes 262144 | tf_op jit(solution)/shard_map/all_to_all | solution.py:205
  15.9 0.1 pad_add_fusion.place_ref
  16.0 19.6 %all-to-all-done = bf16[4,8,16,128]{3,2,1,0:T(8,128)(2,1)S(1)} async-done(((bf16[4,8,16,128]{3,2,1,0:T(8,128)(2,1)}), bf16[4,8,16,128]{3,2,1,0:T(8,128)(2,1)S(1)}, u32[]{:S(2)}, u32[]{:S(2)}) %all-to-all-start) | async-done | bytes 131104 | tf_op jit(solution)/shard_map/all_to_all | solution.py:205
  35.9 50.9 %all-gather.1 = f16[32,520,128]{2,1,0:T(8,128)(2,1)S(1)} all-gather(f16[1,520,128]{2,1,0:T(8,128)(2,1)S(1)} %pad_maximum_fusion), channel_id=1, replica_groups=mesh['z'=16,'x'=4,'c'=2,'y'=4] {'z','c'}, dimensions={0}, use_global_device_ids=true | all-gather | bytes 4392960 | tf_op jit(solution)/shard_map/all_gather | solution.py:213
  86.8 0.0 copy-start
  86.8 0.7 convert_element_type.21
  87.5 0.0 collective-permute-done.refs_1_
  87.5 0.0 collective-permute-done.1.refs_2_
  87.5 0.0 collective-permute-done.2.refs_3_
  87.6 0.3 copy-done
  87.8 4.4 %shard_map.68 = (bf16[2048,256]{1,0:T(8,128)(2,1)}, bf16[2048,256]{1,0:T(8,128)(2,1)}, bf16[16,128,512]{2,1,0:T(8,128)(2,1)S(1)}) custom-call(s32[2]{0:T(128)S(1)} %pad_add_fusion.place_ref, bf16[128,2048]{1,0:T(8,128)(2,1)S(1)} %copy-done, bf16[128,2048]{1,0:T(8,128)(2,1)S(1)} %collective-permute-done.refs_1_, ...), custom_call_target="tpu_custom_call" | custom-call | flops 2147483648 | bytes 16777216 | tf_op jit(solution)/shard_map/pallas_call | solution.py:163
  92.3 19.3 %all_to_all.15 = bf16[16,128,512]{2,1,0:T(8,128)(2,1)S(1)} all-to-all(bf16[16,128,512]{2,1,0:T(8,128)(2,1)S(1)} %get-tuple-element.8), channel_id=1, replica_groups={{0,8,16,24},{1,9,17,25},{2,10,18,26},{3,11,19,27},{4,5,6,7},{12,13,14,1..., dimensions={0} | all-to-all | bytes 4194304 | tf_op jit(solution)/shard_map/all_to_all | solution.py:218
  111.6 0.6 reduce_sum.24
  112.2 9.6 %all_to_all.16 = bf16[4,128,512]{2,1,0:T(8,128)(2,1)S(1)} all-to-all(bf16[4,128,512]{2,1,0:T(8,128)(2,1)S(1)} %reduce_sum.24), channel_id=1, replica_groups={{0,1,2,3},{8,9,10,11},{16,17,18,19},{24,25,26,27},{4,12,20,28},{5,13,21..., dimensions={0} | all-to-all | bytes 1048576 | tf_op jit(solution)/shard_map/all_to_all | solution.py:218
  121.8 0.7 reduce_sum.25
  (9 shorter events, 0.2 us)
Async XLA Ops:
  0.6 86.9 %collective-permute-start = (bf16[128,2048]{1,0:T(8,128)(2,1)}, bf16[128,2048]{1,0:T(8,128)(2,1)S(1)}, u32[]{:S(2)}, u32[]{:S(2)}) collective-permute-start(bf16[128,2048]{1,0:T(8,128)(2,1)} %refs_0_.1), channel_id=1, source_target_pairs={{8,0},{16,8},{24,16},{0,24},{9,1},{17,9},{25,17},{1,25},{10,2},{18... | collective-permute-start | bytes 1572872 | tf_op jit(solution)/shard_map/ppermute | solution.py:207
  5.8 81.7 %collective-permute-start.1 = (bf16[128,2048]{1,0:T(8,128)(2,1)}, bf16[128,2048]{1,0:T(8,128)(2,1)S(1)}, u32[]{:S(2)}, u32[]{:S(2)}) collective-permute-start(bf16[128,2048]{1,0:T(8,128)(2,1)} %refs_0_.1), channel_id=1, source_target_pairs={{16,0},{24,8},{0,16},{8,24},{17,1},{25,9},{1,17},{9,25},{18,2},{26... | collective-permute-start | bytes 1572872 | tf_op jit(solution)/shard_map/ppermute | solution.py:207
  8.3 79.3 %collective-permute-start.2 = (bf16[128,2048]{1,0:T(8,128)(2,1)}, bf16[128,2048]{1,0:T(8,128)(2,1)S(1)}, u32[]{:S(2)}, u32[]{:S(2)}) collective-permute-start(bf16[128,2048]{1,0:T(8,128)(2,1)} %refs_0_.1), channel_id=1, source_target_pairs={{24,0},{0,8},{8,16},{16,24},{25,1},{1,9},{9,17},{17,25},{26,2},{2,... | collective-permute-start | bytes 1572872 | tf_op jit(solution)/shard_map/ppermute | solution.py:207
  12.6 23.0 %all-to-all-start = ((bf16[4,8,16,128]{3,2,1,0:T(8,128)(2,1)}), bf16[4,8,16,128]{3,2,1,0:T(8,128)(2,1)S(1)}, u32[]{:S(2)}, u32[]{:S(2)}) async-start(bf16[4,8,16,128]{3,2,1,0:T(8,128)(2,1)} %shard_map.67), calls=%async_computation | async-start | bytes 262144 | tf_op jit(solution)/shard_map/all_to_all | solution.py:205
  86.8 1.0 copy-start
